TPU v7x, 256 devices: a whole 4x4x8 slice. The times are simulated.
256 devices in a mesh: ep: 16 (over y, x), tp: 16 (over z, core).
Axes of the slice: x: 4, y: 4, z: 8, core: 2. Of those that a mesh axis runs over, the one named last changes fastest.
Arguments:
- tokens: bfloat16 [1024, 4096], P('ep'), may hold values from -6 to 6
- norm_gain: float32 [4096], replicated, may hold values from 0.1 to 1.9
- ffn_gain: float32 [4096], replicated, may hold values from 0.1 to 1.9
- w_in: bfloat16 [4096, 2048], P(None, 'tp'), may hold values from -0.09375 to 0.09375
- decay_rate: float32 [8192], P('tp'), may hold values from 0.02 to 2
- frequency: float32 [8192], P('tp'), may hold values from -3.140625 to 3.140625
- log_step: float32 [128], P('tp'), may hold values from -2.3 to 0
- input_real: float32 [16, 8192], P(None, 'tp'), may hold values from -1 to 1
- input_imag: float32 [16, 8192], P(None, 'tp'), may hold values from -1 to 1
- readout_real: float32 [16, 8192], P(None, 'tp'), may hold values from -0.5 to 0.5
- readout_imag: float32 [16, 8192], P(None, 'tp'), may hold values from -0.5 to 0.5
- skip_gain: float32 [2048], P('tp'), may hold values from -4 to 4
- state_real: float32 [1024, 8192], P('ep', 'tp'), may hold values from -6 to 6
- state_imag: float32 [1024, 8192], P('ep', 'tp'), may hold values from -6 to 6
- w_out: bfloat16 [2048, 4096], P('tp'), may hold values from -0.125 to 0.125
- shared_gate: bfloat16 [4096, 1024], P(None, 'tp'), may hold values from -0.09375 to 0.09375
- shared_up: bfloat16 [4096, 1024], P(None, 'tp'), may hold values from -0.09375 to 0.09375
- shared_down: bfloat16 [1024, 4096], P('tp'), may hold values from -0.1875 to 0.1875
- expert_gate: bfloat16 [64, 4096, 1024], P('ep', 'tp'), may hold values from -0.09375 to 0.09375
- expert_up: bfloat16 [64, 4096, 1024], P('ep', 'tp'), may hold values from -0.09375 to 0.09375
- expert_down: bfloat16 [64, 1024, 4096], P('ep', None, 'tp'), may hold values from -0.1875 to 0.1875
- routing: int32 [1024, 4], P('ep'), may hold values from 0 to 63, all different within a row; in each aligned block of 64 rows (0 to 63, 64 to 127, ...) at most 8 rows name the same one
- route_weight: float32 [1024, 4], P('ep'), may hold values from 0.1 to 1
Outputs:
- mixed: bfloat16 [1024, 4096], P('ep', 'tp')
- new_state_real: float32 [1024, 8192], P('ep', 'tp')
- new_state_imag: float32 [1024, 8192], P('ep', 'tp')
Inputs may be any that keep to these rules, and one draw needn't show every extreme that they name: `routing`: each row names 4 different experts. In the rows of one index of ep (aligned blocks of 64 rows) no expert is named more than 8 times, and in every draw some expert is named exactly 8 times in some block.
All inputs are finite; a program needn't handle non-finite values.
Results may differ from a plain program's by a relative error of at most 0.02.
Values may be sent and summed in bfloat16 or wider, within the bound.
No kernel may reach another device: no remote copies, remote signals or barrier semaphores. Data moves between devices by JAX's collectives and lax.ppermute only.
A program may use at most 64 MiB of HBM per device.

v0:
```python
import jax
import jax.numpy as jnp
from jax import lax
from jax.sharding import PartitionSpec as P

EPS = 1e-06
ROUTED_SCALE = 2.5
HIGH = lax.Precision.HIGHEST


def split_up(x, dim, peers):
    dims = x.shape
    parts = x.reshape(*dims[:dim], peers, dims[dim] // peers, *dims[dim + 1 :])
    return jnp.moveaxis(parts, dim, 0)


def sent_and_summed(x, axis, dim):
    parts = split_up(x, dim, lax.axis_size(axis))
    arrived = lax.all_to_all(parts, axis, split_axis=0, concat_axis=0, tiled=True)
    return arrived.astype(jnp.float32).sum(axis=0)


def sent_to_all(x, axis):
    copies = jnp.broadcast_to(x, (lax.axis_size(axis), *x.shape))
    return lax.all_to_all(copies, axis, split_axis=0, concat_axis=0, tiled=True)


def over_copies(x, axis):
    everything = sent_to_all(x, axis)
    return jnp.sum(everything, axis=0)


def joined_along(parts, dim):
    parts = jnp.moveaxis(parts, 0, dim)
    dims = parts.shape
    return parts.reshape(*dims[:dim], dims[dim] * dims[dim + 1], *dims[dim + 2 :])


def gathered_copies(x, axis, dim):
    return joined_along(sent_to_all(x, axis), dim)


def in_one(arrays, axis):
    line, at, finished = (jnp.concatenate([a.reshape(-1) for a in arrays]), 0, [])
    total = lax.psum(line, axis)
    for a in arrays:
        finished.append(total[at : at + a.size].reshape(a.shape))
        at += a.size
    return tuple(finished)


def rms_scale(values_in, gains):
    values = values_in.astype(jnp.float32)
    factor = lax.rsqrt(jnp.mean(values * values, axis=-1, keepdims=True) + EPS)
    return (values * factor * gains).astype(jnp.bfloat16)


def state_update(
    normed,
    w_in,
    decay_rate,
    frequency,
    log_step,
    input_real,
    input_imag,
    readout_real,
    readout_imag,
    skip_gain,
    state_real,
    state_imag,
):
    seq_count = normed.shape[0]
    groups = log_step.shape[0]
    chan_count = skip_gain.shape[0] // groups
    state_width = decay_rate.shape[0] // groups
    drive_rows = jnp.dot(normed, w_in, preferred_element_type=jnp.float32).astype(jnp.bfloat16)
    drive_f = drive_rows.astype(jnp.float32).reshape(seq_count, groups, chan_count)
    decays = decay_rate.reshape(groups, state_width)
    omegas = frequency.reshape(groups, state_width)
    step_size = jnp.exp(log_step)[:, None]
    pole_mag = jnp.exp(-decays * step_size)
    pole_angle = omegas * step_size
    pole_re = pole_mag * jnp.cos(pole_angle)
    pole_im = pole_mag * jnp.sin(pole_angle)
    pole_norm = decays * decays + omegas * omegas
    diff_re = pole_re - 1.0
    lift_re = (-decays * diff_re + omegas * pole_im) / pole_norm
    lift_im = (-decays * pole_im - omegas * diff_re) / pole_norm
    in_re = input_real.reshape(chan_count, groups, state_width)
    in_im = input_imag.reshape(chan_count, groups, state_width)
    push_re = jnp.einsum("sgh,hgp->sgp", drive_f, in_re, precision=HIGH)
    push_im = jnp.einsum("sgh,hgp->sgp", drive_f, in_im, precision=HIGH)
    old_re = state_real.reshape(seq_count, groups, state_width)
    old_im = state_imag.reshape(seq_count, groups, state_width)
    new_re = pole_re * old_re - pole_im * old_im + lift_re * push_re - lift_im * push_im
    new_im = pole_re * old_im + pole_im * old_re + lift_re * push_im + lift_im * push_re
    out_re = readout_real.reshape(chan_count, groups, state_width)
    out_im = readout_imag.reshape(chan_count, groups, state_width)
    read_rows = jnp.einsum("sgp,hgp->sgh", new_re, out_re, precision=HIGH) - jnp.einsum(
        "sgp,hgp->sgh", new_im, out_im, precision=HIGH
    )
    read_rows = read_rows + skip_gain.reshape(groups, chan_count) * drive_f
    activated = jax.nn.gelu(read_rows).reshape(seq_count, groups * chan_count).astype(jnp.bfloat16)
    return (
        activated,
        new_re.reshape(seq_count, groups * state_width),
        new_im.reshape(seq_count, groups * state_width),
    )


def local(
    tokens,
    norm_gain,
    ffn_gain,
    w_in,
    decay_rate,
    frequency,
    log_step,
    input_real,
    input_imag,
    readout_real,
    readout_imag,
    skip_gain,
    state_real,
    state_imag,
    w_out,
    shared_gate,
    shared_up,
    shared_down,
    expert_gate,
    expert_up,
    expert_down,
    routing,
    route_weight,
):
    seq_count, model_width = tokens.shape
    tp_count = lax.axis_size("tp")
    ep_count = lax.axis_size("ep")
    slice_width = model_width // tp_count
    offset = lax.axis_index("tp") * slice_width
    normed = rms_scale(tokens, norm_gain)
    activated, new_real, new_imag = state_update(
        normed,
        w_in,
        decay_rate,
        frequency,
        log_step,
        input_real,
        input_imag,
        readout_real,
        readout_imag,
        skip_gain,
        state_real,
        state_imag,
    )
    mixer_terms = jnp.dot(activated, w_out, preferred_element_type=jnp.float32)
    mixer_own = sent_and_summed(mixer_terms.astype(jnp.bfloat16), "tp", 1)
    own_tokens = lax.dynamic_slice_in_dim(tokens, offset, slice_width, 1)
    resid_own = (own_tokens.astype(jnp.float32) + mixer_own).astype(jnp.bfloat16)
    resid_f = resid_own.astype(jnp.float32)
    square_sum = over_copies(jnp.sum(resid_f * resid_f, axis=1, keepdims=True), "tp")
    factor = lax.rsqrt(square_sum / model_width + EPS)
    gain_own = lax.dynamic_slice_in_dim(ffn_gain, offset, slice_width, 0)
    rows_own = (resid_f * factor * gain_own).astype(jnp.bfloat16)
    ffn_rows = gathered_copies(rows_own, "tp", 1)
    expert_dev = expert_gate.shape[0]
    expert_count = expert_dev * ep_count
    top_count = routing.shape[1]
    capacity = 2 * seq_count * top_count // expert_count
    slot_count = expert_count * capacity
    flat_ids = routing.reshape(-1)
    one_hot = (flat_ids[:, None] == jnp.arange(expert_count, dtype=jnp.int32)[None, :]).astype(
        jnp.int32
    )
    earlier = jnp.cumsum(one_hot, axis=0) - one_hot
    slot_rank = jnp.sum(earlier * one_hot, axis=1)
    target = flat_ids * capacity + slot_rank
    slot_ids = jnp.arange(slot_count, dtype=jnp.int32)
    placed = (target[None, :] == slot_ids[:, None]).reshape(slot_count, seq_count, top_count)
    dispatch_map = jnp.sum(placed.astype(jnp.float32), axis=2).astype(jnp.bfloat16)
    outgoing = jnp.dot(dispatch_map, rows_own, preferred_element_type=jnp.float32).astype(
        jnp.bfloat16
    )
    outgoing = outgoing.reshape(ep_count, expert_dev * capacity, slice_width)
    incoming = lax.all_to_all(outgoing, "ep", split_axis=0, concat_axis=0, tiled=True)
    arrived = incoming.reshape(ep_count, expert_dev, capacity, slice_width)
    gate_part = jnp.einsum(
        "secd,edf->secf", arrived, expert_gate, preferred_element_type=jnp.float32
    )
    up_part = jnp.einsum("secd,edf->secf", arrived, expert_up, preferred_element_type=jnp.float32)
    gate_full, up_full = tuple(
        (
            part.astype(jnp.float32)
            for part in in_one((gate_part.astype(jnp.bfloat16), up_part.astype(jnp.bfloat16)), "tp")
        )
    )
    inner_rows = (jax.nn.silu(gate_full) * up_full).astype(jnp.bfloat16)
    expert_terms = jnp.einsum(
        "secf,efd->secd", inner_rows, expert_down, preferred_element_type=jnp.float32
    )
    returned = lax.all_to_all(
        expert_terms.reshape(ep_count, expert_dev * capacity, slice_width).astype(jnp.bfloat16),
        "ep",
        split_axis=0,
        concat_axis=0,
        tiled=True,
    ).astype(jnp.float32)
    weights = route_weight / jnp.sum(route_weight, axis=1, keepdims=True) * ROUTED_SCALE
    chosen = target.reshape(seq_count, top_count)[:, :, None] == slot_ids[None, None, :]
    combine = jnp.sum(jnp.where(chosen, weights[:, :, None], 0.0), axis=1)
    routed = jnp.dot(combine, returned.reshape(slot_count, slice_width), precision=HIGH)
    shared_gate_rows = jnp.dot(ffn_rows, shared_gate, preferred_element_type=jnp.float32)
    shared_up_rows = jnp.dot(ffn_rows, shared_up, preferred_element_type=jnp.float32)
    shared_inner = (jax.nn.silu(shared_gate_rows) * shared_up_rows).astype(jnp.bfloat16)
    shared_terms = jnp.dot(shared_inner, shared_down, preferred_element_type=jnp.float32)
    shared_own = sent_and_summed(shared_terms.astype(jnp.bfloat16), "tp", 1)
    mixed = (resid_own.astype(jnp.float32) + shared_own + routed).astype(jnp.bfloat16)
    return (mixed, new_real, new_imag)


def solution(mesh):
    placed = (
        P("ep", None),
        P(),
        P(),
        P(None, "tp"),
        P("tp"),
        P("tp"),
        P("tp"),
        P(None, "tp"),
        P(None, "tp"),
        P(None, "tp"),
        P(None, "tp"),
        P("tp"),
        P("ep", "tp"),
        P("ep", "tp"),
        P("tp", None),
        P(None, "tp"),
        P(None, "tp"),
        P("tp", None),
        P("ep", "tp", None),
        P("ep", "tp", None),
        P("ep", None, "tp"),
        P("ep", None),
        P("ep", None),
    )
    return jax.shard_map(
        local,
        mesh=mesh,
        in_specs=placed,
        out_specs=(P("ep", "tp"), P("ep", "tp"), P("ep", "tp")),
        check_vma=False,
    )
```

profile of v0, /device:TPU:1, one launch (start us, length us, event | category | flops | bytes accessed | tf_op | source)
XLA Modules:
  0.0 237.7 jit_solution(10866147600172250460)
XLA Ops:
  8.1 1.2 fusion.28
  11.7 1.7 convolution_convert_fusion.3
  16.0 1.6 convolution_convert_fusion.1
  18.4 10.0 %all-to-all-start = ((bf16[16,64,256]{2,1,0:T(8,128)(2,1)}), bf16[16,64,256]{2,1,0:T(8,128)(2,1)S(1)}, u32[]{:S(2)}, u32[]{:S(2)}) async-start(bf16[16,64,256]{2,1,0:T(8,128)(2,1)} %bitcast.130), calls=%async_computation | async-start | bytes 1048576 | tf_op jit(solution)/shard_map/all_to_all | solution.py:19
  29.9 15.7 %all-to-all-done = bf16[16,64,256]{2,1,0:T(8,128)(2,1)S(1)} async-done(((bf16[16,64,256]{2,1,0:T(8,128)(2,1)}), bf16[16,64,256]{2,1,0:T(8,128)(2,1)S(1)}, u32[]{:S(2)}, u32[]{:S(2)}) %all-to-all-start) | async-done | bytes 524320 | tf_op jit(solution)/shard_map/all_to_all | solution.py:19
  45.7 0.9 fusion.45
  47.2 3.4 %all-to-all-start.1 = ((f32[16,64,1]{1,2,0:T(1,128)}), f32[16,64,1]{1,2,0:T(1,128)S(1)}, u32[]{:S(2)}, u32[]{:S(2)}) async-start(f32[16,64,1]{1,2,0:T(1,128)} %broadcast_in_dim.12), calls=%async_computation.1 | async-start | bytes 16384 | tf_op jit(solution)/shard_map/all_to_all | solution.py:25
  51.4 5.7 %all-to-all-done.1 = f32[16,64,1]{1,2,0:T(1,128)S(1)} async-done(((f32[16,64,1]{1,2,0:T(1,128)}), f32[16,64,1]{1,2,0:T(1,128)S(1)}, u32[]{:S(2)}, u32[]{:S(2)}) %all-to-all-start.1) | async-done | bytes 4128 | tf_op jit(solution)/shard_map/all_to_all | solution.py:25
  57.5 14.1 %all_to_all.30 = bf16[16,32,256]{2,1,0:T(8,128)(2,1)S(1)} all-to-all(bf16[16,32,256]{2,1,0:T(8,128)(2,1)S(1)} %bitcast.134), channel_id=1, replica_groups=mesh['ep'=16,'tp'=16] {'ep'}, dimensions={0} | all-to-all | bytes 524288 | tf_op jit(solution)/shard_map/all_to_all | solution.py:185
  72.5 5.4 %all-to-all-start.2 = ((bf16[16,64,256]{2,1,0:T(8,128)(2,1)}), bf16[16,64,256]{2,1,0:T(8,128)(2,1)S(1)}, u32[]{:S(2)}, u32[]{:S(2)}) async-start(bf16[16,64,256]{2,1,0:T(8,128)(2,1)} %broadcast_in_dim.13), calls=%async_computation.2 | async-start | bytes 1048576 | tf_op jit(solution)/shard_map/all_to_all | solution.py:25
  78.8 1.2 copy-done.1
  80.8 1.4 pad_maximum_fusion
  84.5 10.7 %all-to-all-done.2 = bf16[16,64,256]{2,1,0:T(8,128)(2,1)S(1)} async-done(((bf16[16,64,256]{2,1,0:T(8,128)(2,1)}), bf16[16,64,256]{2,1,0:T(8,128)(2,1)S(1)}, u32[]{:S(2)}, u32[]{:S(2)}) %all-to-all-start.2) | async-done | bytes 524320 | tf_op jit(solution)/shard_map/all_to_all | solution.py:25
  95.3 1.3 fusion.68
  96.6 2.0 convolution_convert_fusion
  99.5 3.5 %all-to-all-start.3 = ((bf16[16,64,256]{2,1,0:T(8,128)(2,1)}), bf16[16,64,256]{2,1,0:T(8,128)(2,1)S(1)}, u32[]{:S(2)}, u32[]{:S(2)}) async-start(bf16[16,64,256]{2,1,0:T(8,128)(2,1)} %bitcast.119), calls=%async_computation.3 | async-start | bytes 1048576 | tf_op jit(solution)/shard_map/all_to_all | solution.py:19
  102.9 99.2 %all-reduce.2.cloned.1.call-done = bf16[1048576]{0:T(1024)(128)(2,1)} async-done(((bf16[1048576]{0:T(1024)(128)(2,1)}), bf16[1048576]{0:T(1024)(128)(2,1)}) %all-reduce.2.cloned.1.call-update) | async-done | bytes 2097168 | tf_op jit(solution)/shard_map/psum | solution.py:45
  202.2 3.8 %slice_convert_fusion.1 = (f32[524288]{0:T(1024)}, f32[524288]{0:T(1024)}) fusion(bf16[1048576]{0:T(1024)(128)(2,1)} %all-reduce.2.cloned.1.call-done), kind=kLoop, calls=%fused_computation.31 | loop fusion | flops 1048576 | bytes 6291456 | tf_op jit(solution)/shard_map/convert_element_type | solution.py:193
  206.0 2.7 %reshape.311 = f32[16,4,8,1024]{3,2,1,0:T(8,128)} reshape(f32[524288]{0:T(1024)} %get-tuple-element.5) | data formatting | bytes 4194304 | tf_op jit(solution)/shard_map/convert_element_type | solution.py:193
  208.7 2.7 %reshape.312 = f32[16,4,8,1024]{3,2,1,0:T(8,128)} reshape(f32[524288]{0:T(1024)} %get-tuple-element.6) | data formatting | bytes 4194304 | tf_op jit(solution)/shard_map/convert_element_type | solution.py:193
  211.4 3.5 %fusion.21 = bf16[16,4,8,256]{3,2,0,1:T(8,128)(2,1)S(1)} fusion(bf16[4,1024,256]{2,1,0:T(8,128)(2,1)} %param.43, f32[16,4,8,1024]{3,2,1,0:T(8,128)} %reshape.312, f32[16,4,8,1024]{3,2,1,0:T(8,128)} %reshape.311), kind=kOutput, calls=%fused_computation.18 | convolution fusion | flops 271712256 | bytes 6553600 | tf_op jit(solution)/shard_map/secf,efd->secd/dot_general | solution.py:198
  215.7 6.5 %all-to-all-start.5 = ((bf16[16,32,256]{2,1,0:T(8,128)(2,1)}), bf16[16,32,256]{2,1,0:T(8,128)(2,1)S(1)}, u32[]{:S(2)}, u32[]{:S(2)}) async-start(bf16[16,32,256]{2,1,0:T(8,128)(2,1)} %bitcast.122), calls=%async_computation.5 | async-start | bytes 524288 | tf_op jit(solution)/shard_map/all_to_all | solution.py:201
  222.5 7.5 %all-to-all-done.5 = bf16[16,32,256]{2,1,0:T(8,128)(2,1)S(1)} async-done(((bf16[16,32,256]{2,1,0:T(8,128)(2,1)}), bf16[16,32,256]{2,1,0:T(8,128)(2,1)S(1)}, u32[]{:S(2)}, u32[]{:S(2)}) %all-to-all-start.5) | async-done | bytes 262176 | tf_op jit(solution)/shard_map/all_to_all | solution.py:201
  229.9 0.9 fusion.26
  (80 shorter events, 16.5 us)
Async XLA Ops:
  7.2 70.8 %copy-start = (bf16[4,256,1024]{2,1,0:T(8,128)(2,1)S(1)}, bf16[4,256,1024]{2,1,0:T(8,128)(2,1)}, u32[]{:S(2)}) copy-start(bf16[4,256,1024]{2,1,0:T(8,128)(2,1)} %param.42) | copy-start | bytes 6291460
  7.2 6.3 %copy-start.4 = (f32[16,512]{1,0:T(8,128)S(1)}, f32[16,512]{1,0:T(8,128)}, u32[]{:S(2)}) copy-start(f32[16,512]{1,0:T(8,128)} %param.30) | copy-start | bytes 98308
  7.2 6.4 %copy-start.5 = (f32[16,512]{1,0:T(8,128)S(1)}, f32[16,512]{1,0:T(8,128)}, u32[]{:S(2)}) copy-start(f32[16,512]{1,0:T(8,128)} %param.31) | copy-start | bytes 98308
  7.2 6.5 %copy-start.6 = (f32[16,512]{1,0:T(8,128)S(1)}, f32[16,512]{1,0:T(8,128)}, u32[]{:S(2)}) copy-start(f32[16,512]{1,0:T(8,128)} %param.32) | copy-start | bytes 98308
  7.2 6.6 %copy-start.7 = (f32[16,512]{1,0:T(8,128)S(1)}, f32[16,512]{1,0:T(8,128)}, u32[]{:S(2)}) copy-start(f32[16,512]{1,0:T(8,128)} %param.33) | copy-start | bytes 98308
  7.2 6.6 %copy-start.2 = (f32[64,512]{1,0:T(8,128)S(1)}, f32[64,512]{1,0:T(8,128)}, u32[]{:S(2)}) copy-start(f32[64,512]{1,0:T(8,128)} %param.35) | copy-start | bytes 393220
  7.2 6.7 %copy-start.3 = (f32[64,512]{1,0:T(8,128)S(1)}, f32[64,512]{1,0:T(8,128)}, u32[]{:S(2)}) copy-start(f32[64,512]{1,0:T(8,128)} %param.36) | copy-start | bytes 393220
  15.5 12.9 %copy-start.8 = (s32[64,4]{0,1:T(4,128)S(1)}, s32[64,4]{0,1:T(4,128)}, u32[]{:S(2)}) copy-start(s32[64,4]{0,1:T(4,128)} %param.44) | copy-start | bytes 3076
  18.4 27.2 %all-to-all-start = ((bf16[16,64,256]{2,1,0:T(8,128)(2,1)}), bf16[16,64,256]{2,1,0:T(8,128)(2,1)S(1)}, u32[]{:S(2)}, u32[]{:S(2)}) async-start(bf16[16,64,256]{2,1,0:T(8,128)(2,1)} %bitcast.130), calls=%async_computation | async-start | bytes 1048576 | tf_op jit(solution)/shard_map/all_to_all | solution.py:19
  47.2 10.0 %all-to-all-start.1 = ((f32[16,64,1]{1,2,0:T(1,128)}), f32[16,64,1]{1,2,0:T(1,128)S(1)}, u32[]{:S(2)}, u32[]{:S(2)}) async-start(f32[16,64,1]{1,2,0:T(1,128)} %broadcast_in_dim.12), calls=%async_computation.1 | async-start | bytes 16384 | tf_op jit(solution)/shard_map/all_to_all | solution.py:25
  72.5 22.8 %all-to-all-start.2 = ((bf16[16,64,256]{2,1,0:T(8,128)(2,1)}), bf16[16,64,256]{2,1,0:T(8,128)(2,1)S(1)}, u32[]{:S(2)}, u32[]{:S(2)}) async-start(bf16[16,64,256]{2,1,0:T(8,128)(2,1)} %broadcast_in_dim.13), calls=%async_computation.2 | async-start | bytes 1048576 | tf_op jit(solution)/shard_map/all_to_all | solution.py:25
  77.9 124.2 %all-reduce.2.cloned.1.call-start = ((), (), s32[]{:S(2)}) async-start(), calls=%async_computation.6 | async-start | bytes 4194304 | tf_op jit(solution)/shard_map/psum | solution.py:45
  78.4 1.6 copy-start.1
  82.3 0.7 copy-start.9
  99.5 116.2 %all-to-all-start.3 = ((bf16[16,64,256]{2,1,0:T(8,128)(2,1)}), bf16[16,64,256]{2,1,0:T(8,128)(2,1)S(1)}, u32[]{:S(2)}, u32[]{:S(2)}) async-start(bf16[16,64,256]{2,1,0:T(8,128)(2,1)} %bitcast.119), calls=%async_computation.3 | async-start | bytes 1048576 | tf_op jit(solution)/shard_map/all_to_all | solution.py:19
  215.7 14.2 %all-to-all-start.5 = ((bf16[16,32,256]{2,1,0:T(8,128)(2,1)}), bf16[16,32,256]{2,1,0:T(8,128)(2,1)S(1)}, u32[]{:S(2)}, u32[]{:S(2)}) async-start(bf16[16,32,256]{2,1,0:T(8,128)(2,1)} %bitcast.122), calls=%async_computation.5 | async-start | bytes 524288 | tf_op jit(solution)/shard_map/all_to_all | solution.py:201
Sparse Core Ops, SparseCore 0:
  82.4 119.6 all-reduce.1
where the time goes:
time: 239 us; the launch traced here: 238 us
  waiting for transfers between devices  139 us (58%)
  starting transfers between devices  28.8 us (12%)
  local copies, waits for them, and re-layouts  18 us (8%)
  between operations  14.4 us (6%)
  blocking collectives  14.1 us (6%)
  matrix products  14 us (6%)
  other arithmetic  9.5 us (4%)
    psum x1, waiting for transfers between devices, in_one(): total = lax.psum(line, axis)  99.2 us
    all_to_all x2, waiting for transfers between devices, sent_to_all(): return lax.all_to_all(copies, axis, split_axis=0, concat_axis=0, tiled=True)  16.4 us
    all_to_all x2, waiting for transfers between devices, sent_and_summed(): lax.all_to_all(parts, axis, split_axis=0, concat_axis=0, tiled=True)  15.7 us
    all_to_all x1, blocking collectives, local(): lax.all_to_all(outgoing, 'ep', split_axis=0, concat_axis=0, tiled=True)  14.1 us
    all_to_all x2, starting transfers between devices, sent_and_summed(): lax.all_to_all(parts, axis, split_axis=0, concat_axis=0, tiled=True)  13.4 us
    all_to_all x2, starting transfers between devices, sent_to_all(): return lax.all_to_all(copies, axis, split_axis=0, concat_axis=0, tiled=True)  8.81 us
    all_to_all x1, waiting for transfers between devices, local(): lax.all_to_all(expert_terms.reshape(ep_count, expert_dev * capacity, slic...  7.49 us
    all_to_all x1, starting transfers between devices, local(): lax.all_to_all(expert_terms.reshape(ep_count, expert_dev * capacity, slic...  6.53 us
  transfers between devices with their start and end apart: 6, of which 5 were waited for; matrix products, arithmetic and copies ran while one was open for 11% of the time, Pallas kernels for 0%

commit v1 on v0

v1 whole, which is shorter than its diff:
```python
import jax
import jax.numpy as jnp
from jax import lax
from jax.sharding import Mesh
from jax.sharding import PartitionSpec as P

EPS = 1e-06
ROUTED_SCALE = 2.5
HIGH = lax.Precision.HIGHEST
TP = ("z", "c")


def swapped(x):
    return lax.ppermute(x, "c", [(0, 1), (1, 0)])


def sent_to_all(x, axis):
    copies = jnp.broadcast_to(x, (lax.axis_size(axis), *x.shape))
    return lax.all_to_all(copies, axis, split_axis=0, concat_axis=0, tiled=True)


def of_pair(x, which, dim):
    width = x.shape[dim] // 2
    return lax.dynamic_slice_in_dim(x, which * width, width, dim)


def summed_over_tp(parts, c):
    halves = parts.astype(jnp.bfloat16)
    kept = lax.dynamic_index_in_dim(halves, c, 1, keepdims=False)
    given = lax.dynamic_index_in_dim(halves, 1 - c, 1, keepdims=False)
    got = swapped(given)
    both = (kept.astype(jnp.float32) + got.astype(jnp.float32)).astype(jnp.bfloat16)
    arrived = lax.all_to_all(both, "z", split_axis=0, concat_axis=0, tiled=True)
    return arrived.astype(jnp.float32).sum(axis=0)


def rms_scale(values_in, gains):
    values = values_in.astype(jnp.float32)
    factor = lax.rsqrt(jnp.mean(values * values, axis=-1, keepdims=True) + EPS)
    return (values * factor * gains).astype(jnp.bfloat16)


def state_update(
    normed,
    w_in,
    decay_rate,
    frequency,
    log_step,
    input_real,
    input_imag,
    readout_real,
    readout_imag,
    skip_gain,
    state_real,
    state_imag,
):
    seq_count = normed.shape[0]
    groups = log_step.shape[0]
    chan_count = skip_gain.shape[0] // groups
    state_width = decay_rate.shape[0] // groups
    drive_rows = jnp.dot(normed, w_in, preferred_element_type=jnp.float32).astype(jnp.bfloat16)
    drive_f = drive_rows.astype(jnp.float32).reshape(seq_count, groups, chan_count)
    decays = decay_rate.reshape(groups, state_width)
    omegas = frequency.reshape(groups, state_width)
    step_size = jnp.exp(log_step)[:, None]
    pole_mag = jnp.exp(-decays * step_size)
    pole_angle = omegas * step_size
    pole_re = pole_mag * jnp.cos(pole_angle)
    pole_im = pole_mag * jnp.sin(pole_angle)
    pole_norm = decays * decays + omegas * omegas
    diff_re = pole_re - 1.0
    lift_re = (-decays * diff_re + omegas * pole_im) / pole_norm
    lift_im = (-decays * pole_im - omegas * diff_re) / pole_norm
    in_re = input_real.reshape(chan_count, groups, state_width)
    in_im = input_imag.reshape(chan_count, groups, state_width)
    push_re = jnp.einsum("sgh,hgp->sgp", drive_f, in_re, precision=HIGH)
    push_im = jnp.einsum("sgh,hgp->sgp", drive_f, in_im, precision=HIGH)
    old_re = state_real.reshape(seq_count, groups, state_width)
    old_im = state_imag.reshape(seq_count, groups, state_width)
    new_re = pole_re * old_re - pole_im * old_im + lift_re * push_re - lift_im * push_im
    new_im = pole_re * old_im + pole_im * old_re + lift_re * push_im + lift_im * push_re
    out_re = readout_real.reshape(chan_count, groups, state_width)
    out_im = readout_imag.reshape(chan_count, groups, state_width)
    read_rows = jnp.einsum("sgp,hgp->sgh", new_re, out_re, precision=HIGH) - jnp.einsum(
        "sgp,hgp->sgh", new_im, out_im, precision=HIGH
    )
    read_rows = read_rows + skip_gain.reshape(groups, chan_count) * drive_f
    activated = jax.nn.gelu(read_rows).reshape(seq_count, groups * chan_count).astype(jnp.bfloat16)
    return (
        activated,
        new_re.reshape(seq_count, groups * state_width),
        new_im.reshape(seq_count, groups * state_width),
    )


def local(
    tokens,
    norm_gain,
    ffn_gain,
    w_in,
    decay_rate,
    frequency,
    log_step,
    input_real,
    input_imag,
    readout_real,
    readout_imag,
    skip_gain,
    state_real,
    state_imag,
    w_out,
    shared_gate,
    shared_up,
    shared_down,
    expert_gate,
    expert_up,
    expert_down,
    routing,
    route_weight,
):
    bf16, f32 = jnp.bfloat16, jnp.float32
    seq_count, model_width = tokens.shape
    ep_count, z_count = lax.axis_size("ep"), lax.axis_size("z")
    z, c = lax.axis_index("z"), lax.axis_index("c")
    slice_width = model_width // (2 * z_count)
    offset = (2 * z + c) * slice_width
    other_offset = (2 * z + 1 - c) * slice_width

    gate_own, up_own, down_own = (of_pair(w, c, 0) for w in (expert_gate, expert_up, expert_down))
    gate_par, up_par, down_par = (
        swapped(of_pair(w, 1 - c, 0)) for w in (expert_gate, expert_up, expert_down)
    )

    normed = rms_scale(tokens, norm_gain)
    activated, new_real, new_imag = state_update(
        normed,
        w_in,
        decay_rate,
        frequency,
        log_step,
        input_real,
        input_imag,
        readout_real,
        readout_imag,
        skip_gain,
        state_real,
        state_imag,
    )
    mixer_parts = jnp.einsum(
        "sk,kzcd->zcsd",
        activated,
        w_out.reshape(-1, z_count, 2, slice_width),
        preferred_element_type=f32,
    )
    mixer_own = summed_over_tp(mixer_parts, c)
    own_tokens = lax.dynamic_slice_in_dim(tokens, offset, slice_width, 1)
    resid_own = (own_tokens.astype(f32) + mixer_own).astype(bf16)

    expert_dev = expert_gate.shape[0]
    expert_count = expert_dev * ep_count
    top_count = routing.shape[1]
    capacity = 2 * seq_count * top_count // expert_count
    slot_count = expert_count * capacity
    flat_ids = routing.reshape(-1)
    one_hot = (flat_ids[:, None] == jnp.arange(expert_count, dtype=jnp.int32)[None, :]).astype(
        jnp.int32
    )
    earlier = jnp.cumsum(one_hot, axis=0) - one_hot
    slot_rank = jnp.sum(earlier * one_hot, axis=1)
    target = jnp.bitwise_xor(flat_ids, c * (expert_dev // 2)) * capacity + slot_rank
    slot_ids = jnp.arange(slot_count, dtype=jnp.int32)
    placed = (target[None, :] == slot_ids[:, None]).reshape(slot_count, seq_count, top_count)
    dispatch_map = jnp.sum(placed.astype(f32), axis=2).astype(bf16)
    outgoing = jnp.dot(dispatch_map, resid_own, preferred_element_type=f32).astype(bf16)
    outgoing = outgoing.reshape(ep_count, expert_dev * capacity, slice_width)
    incoming = lax.all_to_all(outgoing, "ep", split_axis=0, concat_axis=0, tiled=True)

    along_z = sent_to_all(resid_own, "z")
    across = swapped(along_z)
    first = jnp.where(c == 0, along_z, across)
    second = jnp.where(c == 0, across, along_z)
    resid_rows = jnp.stack([first, second], axis=1)
    resid_rows = resid_rows.transpose(2, 0, 1, 3).reshape(seq_count, model_width)
    ffn_rows = rms_scale(resid_rows, ffn_gain)
    shared_gate_rows = jnp.dot(ffn_rows, shared_gate, preferred_element_type=f32)
    shared_up_rows = jnp.dot(ffn_rows, shared_up, preferred_element_type=f32)
    shared_inner = (jax.nn.silu(shared_gate_rows) * shared_up_rows).astype(bf16)
    shared_parts = jnp.einsum(
        "sf,fzcd->zcsd",
        shared_inner,
        shared_down.reshape(-1, z_count, 2, slice_width),
        preferred_element_type=f32,
    )
    shared_own = summed_over_tp(shared_parts, c)

    half = expert_dev // 2
    pair_rows = half * ep_count * capacity
    arrived = incoming.reshape(ep_count, 2, half, capacity, slice_width)
    rows_own, rows_given = arrived[:, 0], arrived[:, 1]
    rows_par = swapped(rows_given)
    gain_own = lax.dynamic_slice_in_dim(ffn_gain, offset, slice_width, 0)
    gain_par = lax.dynamic_slice_in_dim(ffn_gain, other_offset, slice_width, 0)
    own_f, par_f = rows_own.astype(f32), rows_par.astype(f32)
    squares = jnp.sum(own_f * own_f, axis=-1) + jnp.sum(par_f * par_f, axis=-1)
    squares = squares.transpose(1, 0, 2).reshape(-1)
    squares_high = squares.astype(bf16)
    squares_low = (squares - squares_high.astype(f32)).astype(bf16)
    scaled_own = (own_f * gain_own).astype(bf16)
    scaled_par = (par_f * gain_par).astype(bf16)

    def sums(w_own, w_par):
        def one(rows, w):
            return jnp.einsum("secd,edf->escf", rows, w, preferred_element_type=f32)

        whole = one(scaled_own, w_own) + one(scaled_par, w_par)
        return whole.astype(bf16).reshape(pair_rows, z_count, -1).transpose(1, 0, 2)

    gate_parts, up_parts = sums(gate_own, gate_par), sums(up_own, up_par)
    lanes = gate_parts.shape[2]
    extra = jnp.concatenate([squares_high, squares_low]).reshape(1, -1, lanes)
    extra = jnp.broadcast_to(extra, (z_count, *extra.shape[1:]))
    parcel = jnp.concatenate([gate_parts, up_parts, extra], axis=1)
    parcels = lax.all_to_all(parcel, "z", split_axis=0, concat_axis=0, tiled=True)
    totals = parcels.astype(f32).sum(axis=0)
    squares_all = totals[2 * pair_rows :].reshape(2, pair_rows).sum(axis=0)
    factor = lax.rsqrt(squares_all / model_width + EPS)[:, None]
    gate_rows, up_rows = totals[:pair_rows] * factor, totals[pair_rows : 2 * pair_rows] * factor
    inner = (jax.nn.silu(gate_rows) * up_rows).astype(bf16)
    inner_all = sent_to_all(inner, "z").reshape(z_count, half, -1, lanes)

    def down(w):
        w_f = w.reshape(half, z_count, lanes, slice_width)
        out = jnp.einsum("zerf,ezfd->erd", inner_all, w_f, preferred_element_type=f32)
        out = out.astype(bf16).reshape(half, ep_count, capacity, slice_width)
        return out.transpose(1, 0, 2, 3).reshape(ep_count, half * capacity, slice_width)

    out_own, out_given = down(down_own), down(down_par)
    results = jnp.concatenate([out_own, swapped(out_given)], axis=1)
    returned = lax.all_to_all(results, "ep", split_axis=0, concat_axis=0, tiled=True).astype(f32)

    weights = route_weight / jnp.sum(route_weight, axis=1, keepdims=True) * ROUTED_SCALE
    chosen = target.reshape(seq_count, top_count)[:, :, None] == slot_ids[None, None, :]
    combine = jnp.sum(jnp.where(chosen, weights[:, :, None], 0.0), axis=1)
    routed = jnp.dot(combine, returned.reshape(slot_count, slice_width), precision=HIGH)
    mixed = (resid_own.astype(f32) + shared_own + routed).astype(bf16)
    return (mixed, new_real, new_imag)


def solution(mesh):
    ep_count, tp_count = mesh.devices.shape
    cores = Mesh(mesh.devices.reshape(ep_count, tp_count // 2, 2), ("ep", "z", "c"))
    placed = (
        P("ep", None),
        P(),
        P(),
        P(None, TP),
        P(TP),
        P(TP),
        P(TP),
        P(None, TP),
        P(None, TP),
        P(None, TP),
        P(None, TP),
        P(TP),
        P("ep", TP),
        P("ep", TP),
        P(TP, None),
        P(None, TP),
        P(None, TP),
        P(TP, None),
        P("ep", TP, None),
        P("ep", TP, None),
        P("ep", None, TP),
        P("ep", None),
        P("ep", None),
    )
    return jax.shard_map(
        local,
        mesh=cores,
        in_specs=placed,
        out_specs=(P("ep", TP), P("ep", TP), P("ep", TP)),
        check_vma=False,
    )
```

time: 239 us -> 169 us (0.71)
  waiting for transfers between devices: 139 us -> 51.8 us
  starting transfers between devices: 28.8 us -> 46.2 us
  blocking collectives: 14.1 us -> 0 us
  local copies, waits for them, and re-layouts: 18 us -> 31.9 us
  between operations: 14.4 us -> 1.2 us
  matrix products: 14 us -> 20.8 us
  other arithmetic: 9.5 us -> 15.6 us
    psum x1 -> x0, waiting for transfers between devices: 99.2 us -> none  [in_one(): total = lax.psum(line, axis)]
    all_to_all x3 -> x5, waiting for transfers between devices: 23.2 us -> 44.8 us  [the longest x1 18 us: local(): lax.all_to_all(parcel, 'z', split_axis=0, concat_axis=0, tiled=True)]
    all_to_all x1 -> x0, blocking collectives: 14.1 us -> none  [local(): lax.all_to_all(outgoing, 'ep', split_axis=0, concat_axis=0, tiled=True)]
    ppermute x0 -> x8, starting transfers between devices: none -> 10.9 us  [swapped(): return lax.ppermute(x, 'c', [(0, 1), (1, 0)])]
    all_to_all x2, waiting for transfers between devices: 16.4 us -> 6.9 us  [sent_to_all(): return lax.all_to_all(copies, axis, split_axis=0, concat_axis=0, tiled=True)]
    all_to_all x3 -> x5, starting transfers between devices: 20 us -> 27.1 us  [the longest x2 10 us: summed_over_tp(): arrived = lax.all_to_all(both, 'z', split_axis=0, concat_axis=0, tiled=True)]
    dynamic_slice x1 -> x4, local copies, waits for them, and re-layouts: 0.77 us -> 6.95 us  [the longest x3 6.31 us: of_pair(): return lax.dynamic_slice_in_dim(x, which * width, width, dim)]
    dot_general x7 -> x10, matrix products: 9.56 us -> 14.5 us  [the longest x4 4.98 us: one(): return jnp.einsum('secd,edf->escf', rows, w, preferred_element_type=f32)]
  transfers between devices with their start and end apart: 6 -> 15, of which waited for: 5 -> 6; matrix products, arithmetic and copies ran while one was open for 11% -> 29% of each run, Pallas kernels for 0% -> 0%
where the time goes in v1:
time: 169 us; the launch traced here: 168 us
  waiting for transfers between devices  51.8 us (31%)
  starting transfers between devices  46.2 us (27%)
  local copies, waits for them, and re-layouts  31.9 us (19%)
  matrix products  20.8 us (12%)
  other arithmetic  15.6 us (9%)
    all_to_all x1, waiting for transfers between devices, local(): lax.all_to_all(parcel, 'z', split_axis=0, concat_axis=0, tiled=True)  18 us
    all_to_all x2, waiting for transfers between devices, summed_over_tp(): arrived = lax.all_to_all(both, 'z', split_axis=0, concat_axis=0, tiled=True)  16.7 us
    ppermute x8, starting transfers between devices, swapped(): return lax.ppermute(x, 'c', [(0, 1), (1, 0)])  10.9 us
    all_to_all x2, starting transfers between devices, summed_over_tp(): arrived = lax.all_to_all(both, 'z', split_axis=0, concat_axis=0, tiled=True)  10 us
    all_to_all x2, starting transfers between devices, sent_to_all(): return lax.all_to_all(copies, axis, split_axis=0, concat_axis=0, tiled=True)  8.2 us
    all_to_all x1, waiting for transfers between devices, local(): lax.all_to_all(results, 'ep', split_axis=0, concat_axis=0, tiled=True)  7.93 us
    all_to_all x2, waiting for transfers between devices, sent_to_all(): return lax.all_to_all(copies, axis, split_axis=0, concat_axis=0, tiled=True)  6.9 us
    all_to_all x1, starting transfers between devices, local(): lax.all_to_all(parcel, 'z', split_axis=0, concat_axis=0, tiled=True)  6.8 us
  transfers between devices with their start and end apart: 15, of which 6 were waited for; matrix products, arithmetic and copies ran while one was open for 29% of the time, Pallas kernels for 0%

profile of v1, /device:TPU:1, one launch (start us, length us, event | category | flops | bytes accessed | tf_op | source)
XLA Modules:
  0.0 167.5 jit_solution(14183240588586010712)
XLA Ops:
  4.4 1.8 %convolution_convert_fusion.3 = bf16[64,128]{1,0:T(8,128)(2,1)S(1)} fusion(bf16[4096,128]{1,0:T(8,128)(2,1)} %param.26, bf16[64,4096]{1,0:T(8,128)(2,1)} %param.23, f32[4096]{0:T(1024)} %param.24, f32[64]{0:T(128)S(1)} %add_rsqrt_fusion.2), kind=kOutput, calls=%fused_computation.24 | convolution fusion | flops 68165632 | bytes 1605888 | tf_op jit(solution)/shard_map/dot_general | solution.py:61
  9.6 1.8 %reshape.323 = bf16[128,8,2,256]{3,2,1,0:T(2,128)(2,1)S(1)} reshape(bf16[128,4096]{1,0:T(8,128)(2,1)} %param.37) | data formatting | bytes 2097152 | tf_op jit(solution)/shard_map/reshape | solution.py:152
  18.3 3.3 %collective-permute-start = (bf16[8,64,256]{2,1,0:T(8,128)(2,1)S(1)}, bf16[8,64,256]{2,1,0:T(8,128)(2,1)S(1)}, u32[]{:S(2)}, u32[]{:S(2)}) collective-permute-start(bf16[8,64,256]{2,1,0:T(8,128)(2,1)S(1)} %dynamic-slice_bitcast_fusion.1), channel_id=1, source_target_pairs={{0,1},{1,0},{2,3},{3,2},{4,5},{5,4},{6,7},{7,6},{8,9},{9,8},{10,11... | collective-permute-start | bytes 786440 | tf_op jit(solution)/shard_map/ppermute | solution.py:14
  25.2 6.6 %all-to-all-start = ((bf16[8,64,256]{2,1,0:T(8,128)(2,1)}), bf16[8,64,256]{2,1,0:T(8,128)(2,1)S(1)}, u32[]{:S(2)}, u32[]{:S(2)}) async-start(bf16[8,64,256]{2,1,0:T(8,128)(2,1)} %fusion.28), calls=%async_computation | async-start | bytes 524288 | tf_op jit(solution)/shard_map/all_to_all | solution.py:33
  33.6 9.0 %all-to-all-done = bf16[8,64,256]{2,1,0:T(8,128)(2,1)S(1)} async-done(((bf16[8,64,256]{2,1,0:T(8,128)(2,1)}), bf16[8,64,256]{2,1,0:T(8,128)(2,1)S(1)}, u32[]{:S(2)}, u32[]{:S(2)}) %all-to-all-start) | async-done | bytes 262176 | tf_op jit(solution)/shard_map/all_to_all | solution.py:33
  44.4 6.8 %all-to-all-start.3 = ((bf16[16,32,256]{2,1,0:T(8,128)(2,1)}), bf16[16,32,256]{2,1,0:T(8,128)(2,1)S(1)}, u32[]{:S(2)}, u32[]{:S(2)}) async-start(bf16[16,32,256]{2,1,0:T(8,128)(2,1)} %bitcast.22), calls=%async_computation.3 | async-start | bytes 524288 | tf_op jit(solution)/shard_map/all_to_all | solution.py:176
  51.1 2.3 %constant_dynamic-slice_fusion.2 = bf16[2,256,1024]{2,1,0:T(8,128)(2,1)} fusion(bf16[4,256,1024]{2,1,0:T(8,128)(2,1)} %param.42, s32[]{:T(128)S(6)} %select_n.51), kind=kLoop, calls=%fused_computation.131 | loop fusion | bytes 2097156 | tf_op jit(solution)/shard_map/dynamic_slice | solution.py:24
  53.4 2.3 %collective-permute-start.5 = (bf16[2,256,1024]{2,1,0:T(8,128)(2,1)}, bf16[2,256,1024]{2,1,0:T(8,128)(2,1)}, u32[]{:S(2)}, u32[]{:S(2)}) collective-permute-start(bf16[2,256,1024]{2,1,0:T(8,128)(2,1)} %constant_dynamic-slice_fusion.2), channel_id=1, source_target_pairs={{0,1},{1,0},{2,3},{3,2},{4,5},{5,4},{6,7},{7,6},{8,9},{9,8},{10,11... | collective-permute-start | bytes 3145736 | tf_op jit(solution)/shard_map/ppermute | solution.py:14
  56.4 2.3 %all-to-all-done.3 = bf16[16,32,256]{2,1,0:T(8,128)(2,1)S(1)} async-done(((bf16[16,32,256]{2,1,0:T(8,128)(2,1)}), bf16[16,32,256]{2,1,0:T(8,128)(2,1)S(1)}, u32[]{:S(2)}, u32[]{:S(2)}) %all-to-all-start.3) | async-done | bytes 262176 | tf_op jit(solution)/shard_map/all_to_all | solution.py:176
  59.4 4.1 %all-to-all-start.1 = ((bf16[8,64,256]{2,1,0:T(8,128)(2,1)}), bf16[8,64,256]{2,1,0:T(8,128)(2,1)}, u32[]{:S(2)}, u32[]{:S(2)}) async-start(bf16[8,64,256]{2,1,0:T(8,128)(2,1)} %broadcast_in_dim.14), calls=%async_computation.1 | async-start | bytes 524288 | tf_op jit(solution)/shard_map/all_to_all | solution.py:19
  63.6 3.6 %collective-permute-start.3 = (bf16[16,2,8,256]{3,2,1,0:T(8,128)(2,1)S(1)}, bf16[16,2,8,256]{3,2,1,0:T(8,128)(2,1)S(1)}, u32[]{:S(2)}, u32[]{:S(2)}) collective-permute-start(bf16[16,2,8,256]{3,2,1,0:T(8,128)(2,1)S(1)} %slice_bitcast_fusion), channel_id=1, source_target_pairs={{0,1},{1,0},{2,3},{3,2},{4,5},{5,4},{6,7},{7,6},{8,9},{9,8},{10,11... | collective-permute-start | bytes 393224 | tf_op jit(solution)/shard_map/ppermute | solution.py:14
  71.7 1.9 %fusion = bf16[2,16,8,1024]{3,2,1,0:T(8,128)(2,1)S(1)} fusion(f32[2,16,8,1024]{3,2,1,0:T(8,128)} %fusion.19, bf16[2,256,1024]{2,1,0:T(8,128)(2,1)} %collective-permute-done.4, bf16[16,2,8,256]{3,2,1,0:T(8,128)(2,1)S(1)} %get-tuple-element.13), kind=kOutput, calls=%fused_computation.9 | convolution fusion | flops 134742016 | bytes 2752512 | tf_op jit(solution)/shard_map/secd,edf->escf/dot_general | solution.py:213
  76.6 6.8 %all-to-all-start.4 = ((bf16[8,516,128]{2,1,0:T(8,128)(2,1)}), bf16[8,516,128]{2,1,0:T(8,128)(2,1)}, u32[]{:S(2)}, u32[]{:S(2)}) async-start(bf16[8,516,128]{2,1,0:T(8,128)(2,1)} %pad_maximum_fusion), calls=%async_computation.4 | async-start | bytes 2129920 | tf_op jit(solution)/shard_map/all_to_all | solution.py:223
  83.9 3.0 %constant_dynamic-slice_fusion.1 = (bf16[2,1024,256]{2,1,0:T(8,128)(2,1)}, bf16[2,1024,256]{2,1,0:T(8,128)(2,1)}) fusion(bf16[4,1024,256]{2,1,0:T(8,128)(2,1)} %param.43, s32[]{:T(128)S(6)} %select_n.49, s32[]{:T(128)S(6)} %select_n.51), kind=kLoop, calls=%fused_computation.130 | loop fusion | bytes 4194312 | tf_op jit(solution)/shard_map/dynamic_slice | solution.py:24
  90.1 1.8 %copy.208 = f32[64,8,2,256]{3,2,1,0:T(2,128)} copy(f32[64,8,2,256]{3,0,1,2:T(8,128)S(1)} %convert_bitcast_fusion) | data formatting | bytes 2097152 | tf_op jit(solution)/shard_map/convert_element_type | solution.py:38
  91.9 2.1 %reshape.343 = f32[64,4096]{1,0:T(8,128)S(1)} reshape(f32[64,8,2,256]{3,2,1,0:T(2,128)} %copy.208) | data formatting | bytes 2097152 | tf_op jit(solution)/shard_map/convert_element_type | solution.py:38
  95.2 18.0 %all-to-all-done.4 = bf16[8,516,128]{2,1,0:T(8,128)(2,1)} async-done(((bf16[8,516,128]{2,1,0:T(8,128)(2,1)}), bf16[8,516,128]{2,1,0:T(8,128)(2,1)}, u32[]{:S(2)}, u32[]{:S(2)}) %all-to-all-start.4) | async-done | bytes 1056800 | tf_op jit(solution)/shard_map/all_to_all | solution.py:223
  117.3 4.1 %all-to-all-start.5 = ((bf16[8,256,128]{2,1,0:T(8,128)(2,1)}), bf16[8,256,128]{2,1,0:T(8,128)(2,1)}, u32[]{:S(2)}, u32[]{:S(2)}) async-start(bf16[8,256,128]{2,1,0:T(8,128)(2,1)} %broadcast_in_dim.18), calls=%async_computation.5 | async-start | bytes 1048576 | tf_op jit(solution)/shard_map/all_to_all | solution.py:19
  122.9 2.8 %convolution_convert_fusion.1 = bf16[64,8,2,256]{3,0,2,1:T(8,128)(2,1)} fusion(bf16[4096,64]{0,1:T(8,128)(2,1)} %param.39, bf16[64,8,2,256]{3,2,1,0:T(2,128)(2,1)} %reshape.324, f32[64,64]{1,0:T(8,128)S(1)} %fusion.71, f32[64,4096]{1,0:T(8,128)S(1)} %reshape.343, f32[4096]{0:T(1024)S(1)} %copy-done.14, f32[64]{0:T(128)S(1)} %add_rsqrt_fusion.1), kind=kOutput, calls=%fused_computation.8 | convolution fusion | flops 68182016 | bytes 2654464 | tf_op jit(solution)/shard_map/sf,fzcd->zcsd/dot_general | solution.py:188
  132.5 6.9 %all-to-all-done.5 = bf16[8,256,128]{2,1,0:T(8,128)(2,1)} async-done(((bf16[8,256,128]{2,1,0:T(8,128)(2,1)}), bf16[8,256,128]{2,1,0:T(8,128)(2,1)}, u32[]{:S(2)}, u32[]{:S(2)}) %all-to-all-start.5) | async-done | bytes 524320 | tf_op jit(solution)/shard_map/all_to_all | solution.py:19
  139.4 3.4 %all-to-all-start.2 = ((bf16[8,64,256]{2,1,0:T(8,128)(2,1)}), bf16[8,64,256]{2,1,0:T(8,128)(2,1)S(1)}, u32[]{:S(2)}, u32[]{:S(2)}) async-start(bf16[8,64,256]{2,1,0:T(8,128)(2,1)} %fusion.27), calls=%async_computation.2 | async-start | bytes 524288 | tf_op jit(solution)/shard_map/all_to_all | solution.py:33
  147.3 7.7 %all-to-all-done.2 = bf16[8,64,256]{2,1,0:T(8,128)(2,1)S(1)} async-done(((bf16[8,64,256]{2,1,0:T(8,128)(2,1)}), bf16[8,64,256]{2,1,0:T(8,128)(2,1)S(1)}, u32[]{:S(2)}, u32[]{:S(2)}) %all-to-all-start.2) | async-done | bytes 262176 | tf_op jit(solution)/shard_map/all_to_all | solution.py:33
  155.0 3.5 %all-to-all-start.6 = ((bf16[16,32,256]{2,1,0:T(8,128)(2,1)}), bf16[16,32,256]{2,1,0:T(8,128)(2,1)S(1)}, u32[]{:S(2)}, u32[]{:S(2)}) async-start(bf16[16,32,256]{2,1,0:T(8,128)(2,1)} %pad_maximum_fusion.2), calls=%async_computation.6 | async-start | bytes 524288 | tf_op jit(solution)/shard_map/all_to_all | solution.py:239
  158.7 7.9 %all-to-all-done.6 = bf16[16,32,256]{2,1,0:T(8,128)(2,1)S(1)} async-done(((bf16[16,32,256]{2,1,0:T(8,128)(2,1)}), bf16[16,32,256]{2,1,0:T(8,128)(2,1)S(1)}, u32[]{:S(2)}, u32[]{:S(2)}) %all-to-all-start.6) | async-done | bytes 262176 | tf_op jit(solution)/shard_map/all_to_all | solution.py:239
  (151 shorter events, 52.6 us)
Async XLA Ops:
  0.6 21.0 %copy-start = (bf16[4,256,1024]{2,1,0:T(8,128)(2,1)S(1)}, bf16[4,256,1024]{2,1,0:T(8,128)(2,1)}, u32[]{:S(2)}) copy-start(bf16[4,256,1024]{2,1,0:T(8,128)(2,1)} %param.41) | copy-start | bytes 6291460
  0.7 8.7 %copy-start.18 = (f32[16,512]{1,0:T(8,128)S(1)}, f32[16,512]{1,0:T(8,128)}, u32[]{:S(2)}) copy-start(f32[16,512]{1,0:T(8,128)} %param.33) | copy-start | bytes 98308
  0.7 8.8 %copy-start.24 = (f32[128]{0:T(128)S(1)}, f32[128]{0:T(128)}, u32[]{:S(2)}) copy-start(f32[128]{0:T(128)} %param.34) | copy-start | bytes 1540
  18.3 6.1 %collective-permute-start = (bf16[8,64,256]{2,1,0:T(8,128)(2,1)S(1)}, bf16[8,64,256]{2,1,0:T(8,128)(2,1)S(1)}, u32[]{:S(2)}, u32[]{:S(2)}) collective-permute-start(bf16[8,64,256]{2,1,0:T(8,128)(2,1)S(1)} %dynamic-slice_bitcast_fusion.1), channel_id=1, source_target_pairs={{0,1},{1,0},{2,3},{3,2},{4,5},{5,4},{6,7},{7,6},{8,9},{9,8},{10,11... | collective-permute-start | bytes 786440 | tf_op jit(solution)/shard_map/ppermute | solution.py:14
  22.7 49.0 %collective-permute-start.4 = (bf16[2,256,1024]{2,1,0:T(8,128)(2,1)}, bf16[2,256,1024]{2,1,0:T(8,128)(2,1)}, u32[]{:S(2)}, u32[]{:S(2)}) collective-permute-start(bf16[2,256,1024]{2,1,0:T(8,128)(2,1)} %constant_dynamic-slice_fusion.3), channel_id=1, source_target_pairs={{0,1},{1,0},{2,3},{3,2},{4,5},{5,4},{6,7},{7,6},{8,9},{9,8},{10,11... | collective-permute-start | bytes 3145736 | tf_op jit(solution)/shard_map/ppermute | solution.py:14
  25.2 30.5 %copy-start.14 = (f32[4096]{0:T(1024)S(1)}, f32[4096]{0:T(1024)}, u32[]{:S(2)}) copy-start(f32[4096]{0:T(1024)} %param.25) | copy-start | bytes 49156
  25.2 17.4 %all-to-all-start = ((bf16[8,64,256]{2,1,0:T(8,128)(2,1)}), bf16[8,64,256]{2,1,0:T(8,128)(2,1)S(1)}, u32[]{:S(2)}, u32[]{:S(2)}) async-start(bf16[8,64,256]{2,1,0:T(8,128)(2,1)} %fusion.28), calls=%async_computation | async-start | bytes 524288 | tf_op jit(solution)/shard_map/all_to_all | solution.py:33
  33.5 9.1 %copy-start.19 = (s32[64,4]{0,1:T(4,128)}, s32[64,4]{0,1:T(4,128)S(1)}, u32[]{:S(2)}) copy-start(s32[64,4]{0,1:T(4,128)S(1)} %multiply_add_fusion.1) | copy-start | bytes 3076
  43.4 20.2 %copy-start.10 = (bf16[64,256]{1,0:T(8,128)(2,1)}, bf16[64,256]{1,0:T(8,128)(2,1)S(1)}, u32[]{:S(2)}) copy-start(bf16[64,256]{1,0:T(8,128)(2,1)S(1)} %add_convert_fusion) | copy-start | bytes 98308
  44.4 14.3 %all-to-all-start.3 = ((bf16[16,32,256]{2,1,0:T(8,128)(2,1)}), bf16[16,32,256]{2,1,0:T(8,128)(2,1)S(1)}, u32[]{:S(2)}, u32[]{:S(2)}) async-start(bf16[16,32,256]{2,1,0:T(8,128)(2,1)} %bitcast.22), calls=%async_computation.3 | async-start | bytes 524288 | tf_op jit(solution)/shard_map/all_to_all | solution.py:176
  53.4 20.2 %collective-permute-start.5 = (bf16[2,256,1024]{2,1,0:T(8,128)(2,1)}, bf16[2,256,1024]{2,1,0:T(8,128)(2,1)}, u32[]{:S(2)}, u32[]{:S(2)}) collective-permute-start(bf16[2,256,1024]{2,1,0:T(8,128)(2,1)} %constant_dynamic-slice_fusion.2), channel_id=1, source_target_pairs={{0,1},{1,0},{2,3},{3,2},{4,5},{5,4},{6,7},{7,6},{8,9},{9,8},{10,11... | collective-permute-start | bytes 3145736 | tf_op jit(solution)/shard_map/ppermute | solution.py:14
  59.4 17.2 %all-to-all-start.1 = ((bf16[8,64,256]{2,1,0:T(8,128)(2,1)}), bf16[8,64,256]{2,1,0:T(8,128)(2,1)}, u32[]{:S(2)}, u32[]{:S(2)}) async-start(bf16[8,64,256]{2,1,0:T(8,128)(2,1)} %broadcast_in_dim.14), calls=%async_computation.1 | async-start | bytes 524288 | tf_op jit(solution)/shard_map/all_to_all | solution.py:19
  63.6 5.2 %collective-permute-start.3 = (bf16[16,2,8,256]{3,2,1,0:T(8,128)(2,1)S(1)}, bf16[16,2,8,256]{3,2,1,0:T(8,128)(2,1)S(1)}, u32[]{:S(2)}, u32[]{:S(2)}) collective-permute-start(bf16[16,2,8,256]{3,2,1,0:T(8,128)(2,1)S(1)} %slice_bitcast_fusion), channel_id=1, source_target_pairs={{0,1},{1,0},{2,3},{3,2},{4,5},{5,4},{6,7},{7,6},{8,9},{9,8},{10,11... | collective-permute-start | bytes 393224 | tf_op jit(solution)/shard_map/ppermute | solution.py:14
  76.6 36.6 %all-to-all-start.4 = ((bf16[8,516,128]{2,1,0:T(8,128)(2,1)}), bf16[8,516,128]{2,1,0:T(8,128)(2,1)}, u32[]{:S(2)}, u32[]{:S(2)}) async-start(bf16[8,516,128]{2,1,0:T(8,128)(2,1)} %pad_maximum_fusion), calls=%async_computation.4 | async-start | bytes 2129920 | tf_op jit(solution)/shard_map/all_to_all | solution.py:223
  83.4 4.8 %collective-permute-start.1 = (bf16[8,64,256]{2,1,0:T(8,128)(2,1)}, bf16[8,64,256]{2,1,0:T(8,128)(2,1)S(1)}, u32[]{:S(2)}, u32[]{:S(2)}) collective-permute-start(bf16[8,64,256]{2,1,0:T(8,128)(2,1)} %all-to-all-done.1), channel_id=1, source_target_pairs={{0,1},{1,0},{2,3},{3,2},{4,5},{5,4},{6,7},{7,6},{8,9},{9,8},{10,11... | collective-permute-start | bytes 786440 | tf_op jit(solution)/shard_map/ppermute | solution.py:14
  86.9 55.9 %collective-permute-start.6 = (bf16[2,1024,256]{2,1,0:T(8,128)(2,1)}, bf16[2,1024,256]{2,1,0:T(8,128)(2,1)}, u32[]{:S(2)}, u32[]{:S(2)}) collective-permute-start(bf16[2,1024,256]{2,1,0:T(8,128)(2,1)} %get-tuple-element.6), channel_id=1, source_target_pairs={{0,1},{1,0},{2,3},{3,2},{4,5},{5,4},{6,7},{7,6},{8,9},{9,8},{10,11... | collective-permute-start | bytes 3145736 | tf_op jit(solution)/shard_map/ppermute | solution.py:14
  117.3 22.1 %all-to-all-start.5 = ((bf16[8,256,128]{2,1,0:T(8,128)(2,1)}), bf16[8,256,128]{2,1,0:T(8,128)(2,1)}, u32[]{:S(2)}, u32[]{:S(2)}) async-start(bf16[8,256,128]{2,1,0:T(8,128)(2,1)} %broadcast_in_dim.18), calls=%async_computation.5 | async-start | bytes 1048576 | tf_op jit(solution)/shard_map/all_to_all | solution.py:19
  127.5 3.3 %collective-permute-start.2 = (bf16[8,64,256]{2,1,0:T(8,128)(2,1)}, bf16[8,64,256]{2,1,0:T(8,128)(2,1)}, u32[]{:S(2)}, u32[]{:S(2)}) collective-permute-start(bf16[8,64,256]{2,1,0:T(8,128)(2,1)} %dynamic-slice_bitcast_fusion), channel_id=1, source_target_pairs={{0,1},{1,0},{2,3},{3,2},{4,5},{5,4},{6,7},{7,6},{8,9},{9,8},{10,11... | collective-permute-start | bytes 786440 | tf_op jit(solution)/shard_map/ppermute | solution.py:14
  132.5 12.6 %copy-start.8 = (bf16[2,1024,256]{2,1,0:T(8,128)(2,1)S(1)}, bf16[2,1024,256]{2,1,0:T(8,128)(2,1)}, u32[]{:S(2)}) copy-start(bf16[2,1024,256]{2,1,0:T(8,128)(2,1)} %get-tuple-element.5) | copy-start | bytes 3145732
  139.4 15.5 %all-to-all-start.2 = ((bf16[8,64,256]{2,1,0:T(8,128)(2,1)}), bf16[8,64,256]{2,1,0:T(8,128)(2,1)S(1)}, u32[]{:S(2)}, u32[]{:S(2)}) async-start(bf16[8,64,256]{2,1,0:T(8,128)(2,1)} %fusion.27), calls=%async_computation.2 | async-start | bytes 524288 | tf_op jit(solution)/shard_map/all_to_all | solution.py:33
  144.5 14.0 %copy-start.20 = (s32[64,4]{0,1:T(4,128)S(1)}, s32[64,4]{0,1:T(4,128)}, u32[]{:S(2)}) copy-start(s32[64,4]{0,1:T(4,128)} %copy-done.19) | copy-start | bytes 3076
  144.6 22.1 %copy-start.11 = (bf16[64,256]{1,0:T(8,128)(2,1)S(1)}, bf16[64,256]{1,0:T(8,128)(2,1)}, u32[]{:S(2)}) copy-start(bf16[64,256]{1,0:T(8,128)(2,1)} %copy-done.10) | copy-start | bytes 98308
  144.6 2.0 %collective-permute-start.7 = (bf16[16,16,256]{2,1,0:T(8,128)(2,1)S(1)}, bf16[16,16,256]{2,1,0:T(8,128)(2,1)S(1)}, u32[]{:S(2)}, u32[]{:S(2)}) collective-permute-start(bf16[16,16,256]{2,1,0:T(8,128)(2,1)S(1)} %bitcast.181), channel_id=1, source_target_pairs={{0,1},{1,0},{2,3},{3,2},{4,5},{5,4},{6,7},{7,6},{8,9},{9,8},{10,11... | collective-permute-start | bytes 393224 | tf_op jit(solution)/shard_map/ppermute | solution.py:14
  155.0 11.7 %all-to-all-start.6 = ((bf16[16,32,256]{2,1,0:T(8,128)(2,1)}), bf16[16,32,256]{2,1,0:T(8,128)(2,1)S(1)}, u32[]{:S(2)}, u32[]{:S(2)}) async-start(bf16[16,32,256]{2,1,0:T(8,128)(2,1)} %pad_maximum_fusion.2), calls=%async_computation.6 | async-start | bytes 524288 | tf_op jit(solution)/shard_map/all_to_all | solution.py:239
  (16 other events, 71.6 us)

commit v2 on v1

v2 whole, which is shorter than its diff:
```python
import functools

import jax
import jax.numpy as jnp
from jax import lax
from jax.experimental import pallas as pl
from jax.experimental.pallas import tpu as pltpu
from jax.sharding import Mesh
from jax.sharding import PartitionSpec as P

EPS = 1e-06
ROUTED_SCALE = 2.5
HIGH = lax.Precision.HIGHEST
TP = ("z", "c")
F32, BF16 = jnp.float32, jnp.bfloat16


def swapped(x):
    return lax.ppermute(x, "c", [(0, 1), (1, 0)])


def exchanged(x, axis, bit):
    return lax.ppermute(x, axis, [(i, i ^ bit) for i in range(lax.axis_size(axis))])


def of_pair(x, which, dim):
    width = x.shape[dim] // 2
    return lax.dynamic_slice_in_dim(x, which * width, width, dim)


def of_bit(x, bit):
    return jnp.where(bit == 0, x[0], x[1])


def rms_scale(values_in, gains):
    values = values_in.astype(F32)
    factor = lax.rsqrt(jnp.mean(values * values, axis=-1, keepdims=True) + EPS)
    return (values * factor * gains).astype(BF16)


def dot32(a, b):
    return jnp.dot(a, b, preferred_element_type=F32)


def dot_nt(a, b):
    return lax.dot_general(a, b, (((1,), (1,)), ((), ())), preferred_element_type=F32)


def two_parts(x):
    high = x.astype(BF16)
    return high, (x - high.astype(F32)).astype(BF16)


def cost(flops, moved):
    return pl.CostEstimate(flops=flops, bytes_accessed=moved, transcendentals=0)


def front_kernel(
    core,
    log_step,
    tokens,
    norm_gain,
    w_in,
    decay_rate,
    frequency,
    input_real,
    input_imag,
    readout_real,
    readout_imag,
    skip_gain,
    state_real,
    state_imag,
    w_out,
    new_real,
    new_imag,
    kept,
    given,
):
    groups = log_step.shape[0]
    chan_count, entries = input_real.shape
    channels = skip_gain.shape[1]
    width = entries // groups
    normed = rms_scale(tokens[...], norm_gain[...])
    drive = dot32(normed, w_in[...]).astype(BF16)
    group_of = lax.broadcasted_iota(jnp.int32, (1, entries), 1) // width
    step_size = jnp.zeros((1, entries), F32)
    for g in range(groups):
        step_size = jnp.where(group_of == g, log_step[g], step_size)
    step_size = jnp.exp(step_size)
    decays, omegas = decay_rate[...], frequency[...]
    pole_mag = jnp.exp(-decays * step_size)
    pole_angle = omegas * step_size
    pole_re = pole_mag * jnp.cos(pole_angle)
    pole_im = pole_mag * jnp.sin(pole_angle)
    pole_norm = decays * decays + omegas * omegas
    diff_re = pole_re - 1.0
    lift_re = (-decays * diff_re + omegas * pole_im) / pole_norm
    lift_im = (-decays * pole_im - omegas * diff_re) / pole_norm
    row_group = lax.broadcasted_iota(jnp.int32, (channels, entries), 0) // chan_count
    col_group = lax.broadcasted_iota(jnp.int32, (channels, entries), 1) // width
    same = row_group == col_group

    def spread(block):
        return two_parts(jnp.where(same, jnp.concatenate([block[...]] * groups, axis=0), 0.0))

    def push_of(block):
        high, low = spread(block)
        return dot32(drive, high) + dot32(drive, low)

    push_re, push_im = push_of(input_real), push_of(input_imag)
    old_re, old_im = state_real[...], state_imag[...]
    new_re = pole_re * old_re - pole_im * old_im + lift_re * push_re - lift_im * push_im
    new_im = pole_re * old_im + pole_im * old_re + lift_re * push_im + lift_im * push_re
    new_real[...] = new_re
    new_imag[...] = new_im

    def read_of(state, block):
        (high, low), (block_high, block_low) = two_parts(state), spread(block)
        return dot_nt(high, block_high) + dot_nt(high, block_low) + dot_nt(low, block_high)

    read = read_of(new_re, readout_real) - read_of(new_im, readout_imag)
    read = read + skip_gain[...] * drive.astype(F32)
    bent = jnp.tanh(0.7978845608028654 * (read + 0.044715 * (read * read * read)))
    activated = (0.5 * read * (1.0 + bent)).astype(BF16)
    wide = kept.shape[2]
    for z in range(kept.shape[0]):
        for out, c in ((kept, core[0]), (given, 1 - core[0])):
            at = pl.multiple_of((2 * z + c) * wide, wide)
            out[z] = dot32(activated, w_out[:, pl.ds(at, wide)]).astype(out.dtype)


def front(core, log_step, *arrays):
    tokens, w_out, state = arrays[0], arrays[-1], arrays[-2]
    seqs, model_width = tokens.shape
    z_count = lax.axis_size("z")
    part = (z_count, seqs, model_width // (2 * z_count))
    smem, vmem = pl.BlockSpec(memory_space=pltpu.SMEM), pl.BlockSpec(memory_space=pltpu.VMEM)
    return pl.pallas_call(
        front_kernel,
        out_shape=(
            jax.ShapeDtypeStruct(state.shape, F32),
            jax.ShapeDtypeStruct(state.shape, F32),
            jax.ShapeDtypeStruct(part, F32),
            jax.ShapeDtypeStruct(part, BF16),
        ),
        in_specs=[smem, smem] + [vmem] * len(arrays),
        out_specs=(vmem,) * 4,
        cost_estimate=cost(4 * seqs * model_width * w_out.shape[0], 2 * w_out.size * 2),
        name="front",
    )(core, log_step, *arrays)


def gate_up_kernel(core, own, par, gain_own, gain_par, gate_own, gate_par, up_own, up_par, parcel):
    e = pl.program_id(0)
    seq_devs, _, _, capacity, width = own.shape
    rows = seq_devs * capacity
    z_count, _, lanes = parcel.shape
    ones = jnp.ones((8, width), BF16)
    squares = jnp.zeros((8, rows), F32)
    scaled = []
    for part, gain in ((own, gain_own), (par, gain_par)):
        values = part[...].reshape(rows, width).astype(F32)
        scaled.append((values * gain[...]).astype(BF16))
        high, low = two_parts(values * values)
        squares = squares + dot_nt(ones, high) + dot_nt(ones, low)
    for at, w_own, w_par in ((0, gate_own, gate_par), (2 * rows, up_own, up_par)):
        sums = dot32(scaled[0], w_own[0]) + dot32(scaled[1], w_par[0])
        sums = sums.astype(BF16)
        for z in range(z_count):
            parcel[z, pl.ds(at + e * rows, rows), :] = sums[:, z * lanes : (z + 1) * lanes]
    high, low = two_parts(squares)
    line = lax.broadcasted_iota(jnp.int32, squares.shape, 0)
    both = jnp.where(line == 0, high.astype(F32), jnp.where(line == 1, low.astype(F32), 0.0))
    for z in range(z_count):
        parcel[z, pl.ds(4 * rows + e * 8, 8), :] = both.astype(BF16)


def gate_up(core, incoming, par, gain_own, gain_par, gate, gate_par, up, up_par):
    seq_devs, _, half, capacity, width = incoming.shape
    z_count = lax.axis_size("z")
    rows, units = seq_devs * capacity, gate.shape[2]
    lanes = units // z_count
    mine = pl.BlockSpec((1, width, units), lambda e, c: (half * c[0] + e, 0, 0))
    theirs = pl.BlockSpec((1, width, units), lambda e, c: (e, 0, 0))
    block = (seq_devs, 1, 1, capacity, width)
    gain = pl.BlockSpec((1, width), lambda e, c: (0, 0))
    depth = 2 * half * rows + half * 8
    return pl.pallas_call(
        gate_up_kernel,
        grid_spec=pltpu.PrefetchScalarGridSpec(
            num_scalar_prefetch=1,
            grid=(half,),
            in_specs=[
                pl.BlockSpec(block, lambda e, c: (0, 0, e, 0, 0)),
                pl.BlockSpec(block, lambda e, c: (0, 0, e, 0, 0)),
                gain,
                gain,
                mine,
                theirs,
                mine,
                theirs,
            ],
            out_specs=pl.BlockSpec((z_count, depth, lanes), lambda e, c: (0, 0, 0)),
        ),
        out_shape=jax.ShapeDtypeStruct((z_count, depth, lanes), BF16),
        cost_estimate=cost(8 * half * rows * width * units, 8 * half * width * units),
        name="gate_up",
    )(core, incoming, par, gain_own, gain_par, gate, gate_par, up, up_par)


def inner_kernel(model_width, half, parcels, inner):
    totals = parcels[0].astype(F32)
    z_count = parcels.shape[0]
    for z in range(1, z_count):
        totals = totals + parcels[z].astype(F32)
    lanes = totals.shape[1]
    pair_rows = inner.shape[1]
    rows = pair_rows // half
    for e in range(half):
        line = 2 * pair_rows + 8 * e
        squares = totals[line : line + 1] + totals[line + 1 : line + 2]
        factor = lax.rsqrt(squares / model_width + EPS)
        factor = jnp.broadcast_to(factor, (lanes, rows)).T
        gate = totals[e * rows : (e + 1) * rows] * factor
        up = totals[pair_rows + e * rows : pair_rows + (e + 1) * rows] * factor
        done = (gate / (1.0 + jnp.exp(-gate)) * up).astype(BF16)
        for z in range(z_count):
            inner[z, e * rows : (e + 1) * rows, :] = done


def inner_copies(parcels, model_width, half):
    z_count, depth, lanes = parcels.shape
    pair_rows = (depth - half * 8) // 2
    return pl.pallas_call(
        functools.partial(inner_kernel, model_width, half),
        out_shape=jax.ShapeDtypeStruct((z_count, pair_rows, lanes), BF16),
        in_specs=[pl.BlockSpec(memory_space=pltpu.VMEM)],
        out_specs=pl.BlockSpec(memory_space=pltpu.VMEM),
        cost_estimate=cost(parcels.size * 4, parcels.size * 4),
        name="inner",
    )(parcels)


def down_kernel(core, inner, down_own, down_par, own, given):
    z_count = inner.shape[0]
    row = jnp.concatenate([inner[z] for z in range(z_count)], axis=1)
    for out, w in ((own, down_own), (given, down_par)):
        out[...] = dot32(row, w[0]).astype(BF16).reshape(out.shape)


def down(core, inner, w_down, w_par, seq_devs, capacity):
    half = w_par.shape[0]
    z_count, pair_rows, lanes = inner.shape
    units, width = w_par.shape[1:]
    rows = pair_rows // half
    out = pl.BlockSpec((seq_devs, capacity, width), lambda e, c: (0, e, 0))
    shape = jax.ShapeDtypeStruct((seq_devs, half * capacity, width), BF16)
    return pl.pallas_call(
        down_kernel,
        grid_spec=pltpu.PrefetchScalarGridSpec(
            num_scalar_prefetch=1,
            grid=(half,),
            in_specs=[
                pl.BlockSpec((z_count, rows, lanes), lambda e, c: (0, e, 0)),
                pl.BlockSpec((1, units, width), lambda e, c: (half * c[0] + e, 0, 0)),
                pl.BlockSpec((1, units, width), lambda e, c: (e, 0, 0)),
            ],
            out_specs=(out, out),
        ),
        out_shape=(shape, shape),
        cost_estimate=cost(4 * half * rows * units * width, 4 * half * units * width),
        name="down",
    )(core, inner, w_down, w_par)


def local(
    tokens,
    norm_gain,
    ffn_gain,
    w_in,
    decay_rate,
    frequency,
    log_step,
    input_real,
    input_imag,
    readout_real,
    readout_imag,
    skip_gain,
    state_real,
    state_imag,
    w_out,
    shared_gate,
    shared_up,
    shared_down,
    expert_gate,
    expert_up,
    expert_down,
    routing,
    route_weight,
):
    seq_count, model_width = tokens.shape
    ep_count, z_count = lax.axis_size("ep"), lax.axis_size("z")
    z, c = lax.axis_index("z"), lax.axis_index("c")
    core = c.reshape(1)
    slice_width = model_width // (2 * z_count)
    offset = (2 * z + c) * slice_width
    other_offset = (2 * z + 1 - c) * slice_width

    gate_par, up_par, down_par = (
        swapped(of_pair(w, 1 - c, 0)) for w in (expert_gate, expert_up, expert_down)
    )

    new_real, new_imag, kept, given = front(
        core,
        log_step,
        tokens,
        norm_gain.reshape(1, -1),
        w_in,
        decay_rate.reshape(1, -1),
        frequency.reshape(1, -1),
        input_real,
        input_imag,
        readout_real,
        readout_imag,
        skip_gain.reshape(1, -1),
        state_real,
        state_imag,
        w_out,
    )
    both = (kept + swapped(given).astype(F32)).astype(BF16)
    mixer_own = lax.all_to_all(both, "z", split_axis=0, concat_axis=0, tiled=True)
    mixer_own = mixer_own.astype(F32).sum(axis=0)
    own_tokens = lax.dynamic_slice_in_dim(tokens, offset, slice_width, 1)
    resid_own = (own_tokens.astype(F32) + mixer_own).astype(BF16)

    expert_dev = expert_gate.shape[0]
    expert_count = expert_dev * ep_count
    top_count = routing.shape[1]
    capacity = 2 * seq_count * top_count // expert_count
    slot_count = expert_count * capacity
    flat_ids = routing.reshape(-1)
    one_hot = (flat_ids[:, None] == jnp.arange(expert_count, dtype=jnp.int32)[None, :]).astype(
        jnp.int32
    )
    earlier = jnp.cumsum(one_hot, axis=0) - one_hot
    slot_rank = jnp.sum(earlier * one_hot, axis=1)
    target = jnp.bitwise_xor(flat_ids, c * (expert_dev // 2)) * capacity + slot_rank
    slot_ids = jnp.arange(slot_count, dtype=jnp.int32)
    placed = (target[None, :] == slot_ids[:, None]).reshape(slot_count, seq_count, top_count)
    dispatch_map = jnp.sum(placed.astype(F32), axis=2).astype(BF16)
    outgoing = jnp.dot(dispatch_map, resid_own, preferred_element_type=F32).astype(BF16)
    outgoing = outgoing.reshape(ep_count, expert_dev * capacity, slice_width)
    incoming = lax.all_to_all(outgoing, "ep", split_axis=0, concat_axis=0, tiled=True)

    half = expert_dev // 2
    arrived = incoming.reshape(ep_count, 2, half, capacity, slice_width)
    parcel = gate_up(
        core,
        arrived,
        swapped(arrived[:, 1:]),
        lax.dynamic_slice_in_dim(ffn_gain, offset, slice_width, 0).reshape(1, -1),
        lax.dynamic_slice_in_dim(ffn_gain, other_offset, slice_width, 0).reshape(1, -1),
        expert_gate,
        gate_par,
        expert_up,
        up_par,
    )
    parcels = lax.all_to_all(parcel, "z", split_axis=0, concat_axis=0, tiled=True)
    copies = inner_copies(parcels, model_width, half)
    inner_all = lax.all_to_all(copies, "z", split_axis=0, concat_axis=0, tiled=True)
    out_own, out_given = down(core, inner_all, expert_down, down_par, ep_count, capacity)
    results = jnp.concatenate([out_own, swapped(out_given)], axis=1)
    returned = lax.all_to_all(results, "ep", split_axis=0, concat_axis=0, tiled=True).astype(F32)

    grown = resid_own[None]
    bit = 1
    while bit < z_count:
        theirs = exchanged(grown, "z", bit)
        low = (z & bit) == 0
        grown = jnp.stack([jnp.where(low, grown, theirs), jnp.where(low, theirs, grown)])
        grown = grown.reshape(-1, seq_count, slice_width)
        bit *= 2
    across = swapped(grown)
    first, second = jnp.where(c == 0, grown, across), jnp.where(c == 0, across, grown)
    resid_rows = jnp.stack([first, second], axis=1)
    resid_rows = resid_rows.transpose(2, 0, 1, 3).reshape(seq_count, model_width)
    ffn_rows = rms_scale(resid_rows, ffn_gain)
    shared_gate_rows, shared_up_rows = dot32(ffn_rows, shared_gate), dot32(ffn_rows, shared_up)
    shared_inner = (jax.nn.silu(shared_gate_rows) * shared_up_rows).astype(BF16)
    shared_parts = jnp.einsum(
        "sf,fzcd->czsd",
        shared_inner,
        shared_down.reshape(-1, z_count, 2, slice_width),
        preferred_element_type=F32,
    )
    shared_own = of_bit(shared_parts, c)
    shared_own = shared_own + swapped(of_bit(shared_parts, 1 - c).astype(BF16)).astype(F32)
    bit = z_count // 2
    while bit > 0:
        halves = shared_own.reshape(2, -1, seq_count, slice_width)
        high = (z & bit) // bit
        theirs = exchanged(of_bit(halves, 1 - high).astype(BF16), "z", bit)
        shared_own = of_bit(halves, high) + theirs.astype(F32)
        bit //= 2
    shared_own = shared_own[0]

    weights = route_weight / jnp.sum(route_weight, axis=1, keepdims=True) * ROUTED_SCALE
    chosen = target.reshape(seq_count, top_count)[:, :, None] == slot_ids[None, None, :]
    combine = jnp.sum(jnp.where(chosen, weights[:, :, None], 0.0), axis=1)
    routed = jnp.dot(combine, returned.reshape(slot_count, slice_width), precision=HIGH)
    mixed = (resid_own.astype(F32) + shared_own + routed).astype(BF16)
    return (mixed, new_real, new_imag)


def solution(mesh):
    ep_count, tp_count = mesh.devices.shape
    cores = Mesh(mesh.devices.reshape(ep_count, tp_count // 2, 2), ("ep", "z", "c"))
    placed = (
        P("ep", None),
        P(),
        P(),
        P(None, TP),
        P(TP),
        P(TP),
        P(TP),
        P(None, TP),
        P(None, TP),
        P(None, TP),
        P(None, TP),
        P(TP),
        P("ep", TP),
        P("ep", TP),
        P(TP, None),
        P(None, TP),
        P(None, TP),
        P(TP, None),
        P("ep", TP, None),
        P("ep", TP, None),
        P("ep", None, TP),
        P("ep", None),
        P("ep", None),
    )
    return jax.shard_map(
        local,
        mesh=cores,
        in_specs=placed,
        out_specs=(P("ep", TP), P("ep", TP), P("ep", TP)),
        check_vma=False,
    )
```

time: 169 us -> 155 us (0.917)
  local copies, waits for them, and re-layouts: 31.9 us -> 12.6 us
  matrix products: 20.8 us -> 5.11 us
  Pallas kernels: 0 us -> 13 us
  waiting for transfers between devices: 51.8 us -> 64.6 us
  other arithmetic: 15.6 us -> 4.99 us
  starting transfers between devices: 46.2 us -> 52.3 us
    ppermute x0 -> x6, waiting for transfers between devices: none -> 27.7 us  [exchanged(): lax.ppermute(x, axis, [(i, i ^ bit) for i in range(lax.axis_size(axis))])]
    all_to_all x4 -> x2, waiting for transfers between devices: 23.5 us -> 6.69 us  [the longest x1 6.69 us: local(): lax.all_to_all(both, 'z', split_axis=0, concat_axis=0, tiled=True)]
    dot_general x15 -> x3, matrix products: 20 us -> 4.22 us  [the longest x1 1.87 us: local(): jnp.einsum('sf,fzcd->czsd', shared_inner, shared_down.reshape(-1, z_count...]
    pallas_call x0 -> x4, Pallas kernels: none -> 13 us  [the longest x1 4.28 us: front(): pl.pallas_call(front_kernel, out_shape=(jax.ShapeDtypeStruct(state.shape,...]
    reshape x14 -> x0, local copies, waits for them, and re-layouts: 8.73 us -> none  [the longest x1 1.83 us: local(): w_out.reshape(-1, z_count, 2, slice_width)]
    all_to_all x4 -> x2, starting transfers between devices: 18.2 us -> 9.97 us  [the longest x1 6.48 us: local(): lax.all_to_all(both, 'z', split_axis=0, concat_axis=0, tiled=True)]
    ppermute x8, starting transfers between devices: 10.9 us -> 18.6 us  [swapped(): return lax.ppermute(x, 'c', [(0, 1), (1, 0)])]
    ppermute x0 -> x6, starting transfers between devices: none -> 6.54 us  [exchanged(): lax.ppermute(x, axis, [(i, i ^ bit) for i in range(lax.axis_size(axis))])]
  transfers between devices with their start and end apart: 15 -> 19, of which waited for: 6 -> 10; matrix products, arithmetic and copies ran while one was open for 29% -> 12% of each run, Pallas kernels for 0% -> 6%
where the time goes in v2:
time: 155 us; the launch traced here: 154 us
  waiting for transfers between devices  64.6 us (42%)
  starting transfers between devices  52.3 us (34%)
  Pallas kernels  13 us (8%)
  local copies, waits for them, and re-layouts  12.6 us (8%)
  matrix products  5.11 us (3%)
  other arithmetic  4.99 us (3%)
    ppermute x6, waiting for transfers between devices, exchanged(): lax.ppermute(x, axis, [(i, i ^ bit) for i in range(lax.axis_size(axis))])  27.7 us
    all_to_all x1, waiting for transfers between devices, local(): lax.all_to_all(parcel, 'z', split_axis=0, concat_axis=0, tiled=True)  22.4 us
    ppermute x8, starting transfers between devices, swapped(): return lax.ppermute(x, 'c', [(0, 1), (1, 0)])  18.6 us
    all_to_all x1, starting transfers between devices, local(): lax.all_to_all(parcel, 'z', split_axis=0, concat_axis=0, tiled=True)  6.92 us
    all_to_all x1, starting transfers between devices, local(): lax.all_to_all(outgoing, 'ep', split_axis=0, concat_axis=0, tiled=True)  6.75 us
    all_to_all x1, waiting for transfers between devices, local(): lax.all_to_all(both, 'z', split_axis=0, concat_axis=0, tiled=True)  6.69 us
    ppermute x6, starting transfers between devices, exchanged(): lax.ppermute(x, axis, [(i, i ^ bit) for i in range(lax.axis_size(axis))])  6.54 us
    all_to_all x1, starting transfers between devices, local(): lax.all_to_all(both, 'z', split_axis=0, concat_axis=0, tiled=True)  6.48 us
  transfers between devices with their start and end apart: 19, of which 10 were waited for; matrix products, arithmetic and copies ran while one was open for 12% of the time, Pallas kernels for 6%

profile of v2, /device:TPU:1, one launch (start us, length us, event | category | flops | bytes accessed | tf_op | source)
XLA Modules:
  0.0 153.7 jit_solution(8329269766563227661)
XLA Ops:
  0.7 4.3 %front.1 = (f32[64,512]{1,0:T(8,128)}, f32[64,512]{1,0:T(8,128)}, f32[8,64,256]{2,1,0:T(8,128)}, bf16[8,64,256]{2,1,0:T(8,128)(2,1)}) custom-call(s32[1]{0:T(128)} %bitcast.core, f32[8]{0:T(128)} %log_step.1, bf16[64,4096]{1,0:T(8,128)(2,1)} %tokens.1, f32[1,4096]{1,0:T(1,128)} %bitcast.104, bf16[4096,128]{1,0:T(8,128)(2,1)} %w_in.1, f32[1,512]{1,0:T(1,128)} %bitcast.107, ...), custom_call_target="tpu_custom_call" | custom-call | flops 134217728 | bytes 2097152 | tf_op jit(solution)/shard_map/front/pallas_call | solution.py:138
  5.0 3.3 %collective-permute-start = (bf16[8,64,256]{2,1,0:T(8,128)(2,1)}, bf16[8,64,256]{2,1,0:T(8,128)(2,1)S(1)}, u32[]{:S(2)}, u32[]{:S(2)}) collective-permute-start(bf16[8,64,256]{2,1,0:T(8,128)(2,1)} %get-tuple-element.10), channel_id=1, source_target_pairs={{0,1},{1,0},{2,3},{3,2},{4,5},{5,4},{6,7},{7,6},{8,9},{9,8},{10,11... | collective-permute-start | bytes 786440 | tf_op jit(solution)/shard_map/ppermute | solution.py:19
  10.4 6.5 %all-to-all-start = ((bf16[8,64,256]{2,1,0:T(8,128)(2,1)}), bf16[8,64,256]{2,1,0:T(8,128)(2,1)S(1)}, u32[]{:S(2)}, u32[]{:S(2)}) async-start(bf16[8,64,256]{2,1,0:T(8,128)(2,1)} %add_convert_fusion), calls=%async_computation | async-start | bytes 524288 | tf_op jit(solution)/shard_map/all_to_all | solution.py:331
  16.8 2.3 %constant_dynamic-slice_fusion.1 = bf16[2,256,1024]{2,1,0:T(8,128)(2,1)} fusion(bf16[4,256,1024]{2,1,0:T(8,128)(2,1)} %up_own.1, s32[]{:T(128)S(6)} %select_n.164), kind=kLoop, calls=%fused_computation.62 | loop fusion | bytes 2097156 | tf_op jit(solution)/shard_map/dynamic_slice | solution.py:28
  21.3 6.7 %all-to-all-done = bf16[8,64,256]{2,1,0:T(8,128)(2,1)S(1)} async-done(((bf16[8,64,256]{2,1,0:T(8,128)(2,1)}), bf16[8,64,256]{2,1,0:T(8,128)(2,1)S(1)}, u32[]{:S(2)}, u32[]{:S(2)}) %all-to-all-start) | async-done | bytes 262176 | tf_op jit(solution)/shard_map/all_to_all | solution.py:331
  28.9 2.7 %collective-permute-done.1 = bf16[1,64,256]{2,1,0:T(8,128)(2,1)S(1)} collective-permute-done((bf16[1,64,256]{2,1,0:T(8,128)(2,1)S(1)}, bf16[1,64,256]{2,1,0:T(8,128)(2,1)S(1)}, u32[]{:S(2)}, u32[]{:S(2)}) %collective-permute-start.1) | collective-permute-done | bytes 32800 | tf_op jit(solution)/shard_map/ppermute | solution.py:23
  31.9 4.3 %collective-permute-done.2 = bf16[2,64,256]{2,1,0:T(8,128)(2,1)S(1)} collective-permute-done((bf16[2,64,256]{2,1,0:T(8,128)(2,1)S(1)}, bf16[2,64,256]{2,1,0:T(8,128)(2,1)S(1)}, u32[]{:S(2)}, u32[]{:S(2)}) %collective-permute-start.2) | collective-permute-done | bytes 65568 | tf_op jit(solution)/shard_map/ppermute | solution.py:23
  38.0 6.8 %all-to-all-start.1 = ((bf16[16,32,256]{2,1,0:T(8,128)(2,1)}), bf16[16,32,256]{2,1,0:T(8,128)(2,1)S(1)}, u32[]{:S(2)}, u32[]{:S(2)}) async-start(bf16[16,32,256]{2,1,0:T(8,128)(2,1)} %bitcast.27), calls=%async_computation.1 | async-start | bytes 524288 | tf_op jit(solution)/shard_map/all_to_all | solution.py:353
  44.8 6.3 %collective-permute-start.4 = (bf16[8,64,256]{2,1,0:T(8,128)(2,1)S(1)}, bf16[8,64,256]{2,1,0:T(8,128)(2,1)S(1)}, u32[]{:S(2)}, u32[]{:S(2)}) collective-permute-start(bf16[8,64,256]{2,1,0:T(8,128)(2,1)S(1)} %bitcast.101), channel_id=1, source_target_pairs={{0,1},{1,0},{2,3},{3,2},{4,5},{5,4},{6,7},{7,6},{8,9},{9,8},{10,11... | collective-permute-start | bytes 786440 | tf_op jit(solution)/shard_map/ppermute | solution.py:19
  53.0 6.5 %collective-permute-start.9 = (bf16[16,1,2,8,256]{4,3,2,1,0:T(8,128)(2,1)}, bf16[16,1,2,8,256]{4,3,2,1,0:T(8,128)(2,1)}, u32[]{:S(2)}, u32[]{:S(2)}) collective-permute-start(bf16[16,1,2,8,256]{4,3,2,1,0:T(8,128)(2,1)} %slice.67), channel_id=1, source_target_pairs={{0,1},{1,0},{2,3},{3,2},{4,5},{5,4},{6,7},{7,6},{8,9},{9,8},{10,11... | collective-permute-start | bytes 393224 | tf_op jit(solution)/shard_map/ppermute | solution.py:19
  59.5 2.2 %reshape.133 = bf16[64,8,2,256]{3,2,1,0:T(2,128)(2,1)} reshape(bf16[64,4096]{1,0:T(8,128)(2,1)} %param.40) | data formatting | bytes 1048576 | tf_op jit(solution)/shard_map/reshape | solution.py:393
  63.7 3.8 %gate_up.1 = bf16[8,528,128]{2,1,0:T(8,128)(2,1)} custom-call(s32[1]{0:T(128)} %bitcast.core, bf16[16,2,2,8,256]{4,3,2,1,0:T(8,128)(2,1)} %bitcast.99, bf16[16,1,2,8,256]{4,3,2,1,0:T(8,128)(2,1)} %collective-permute-done.9.par, f32[1,256]{1,0:T(1,128)} %bitcast.106, f32[1,256]{1,0:T(1,128)} %bitcast.105, bf16[4,256,1024]{2,1,0:T(8,128)(2,1)} %gate_own.1, ...), custom_call_target="tpu_custom_call" | custom-call | flops 536870912 | bytes 4194304 | tf_op jit(solution)/shard_map/gate_up/pallas_call | solution.py:188
  67.5 6.9 %all-to-all-start.2 = ((bf16[8,528,128]{2,1,0:T(8,128)(2,1)}), bf16[8,528,128]{2,1,0:T(8,128)(2,1)}, u32[]{:S(2)}, u32[]{:S(2)}) async-start(bf16[8,528,128]{2,1,0:T(8,128)(2,1)} %gate_up.1), calls=%async_computation.2 | async-start | bytes 2162688 | tf_op jit(solution)/shard_map/all_to_all | solution.py:368
  77.9 1.9 %convolution_bitcast_fusion = f32[2,8,64,256]{3,2,0,1:T(8,128)S(1)} fusion(bf16[4096,64]{0,1:T(8,128)(2,1)S(1)} %copy-done, bf16[64,8,2,256]{3,2,1,0:T(2,128)(2,1)} %reshape.133, f32[64,64]{1,0:T(8,128)S(1)} %fusion.21, f32[64,4096]{1,0:T(8,128)S(1)} %reshape.140, f32[4096]{0:T(1024)S(1)} %copy-done.7, f32[64]{0:T(128)S(1)} %add_rsqrt_fusion), kind=kOutput, calls=%fused_computation | convolution fusion | flops 67919872 | bytes 3178752 | tf_op jit(solution)/shard_map/sf,fzcd->czsd/dot_general | solution.py:390
  82.1 22.4 %all-to-all-done.2.parcels = bf16[8,528,128]{2,1,0:T(8,128)(2,1)} async-done(((bf16[8,528,128]{2,1,0:T(8,128)(2,1)}), bf16[8,528,128]{2,1,0:T(8,128)(2,1)}, u32[]{:S(2)}, u32[]{:S(2)}) %all-to-all-start.2) | async-done | bytes 1081376 | tf_op jit(solution)/shard_map/all_to_all | solution.py:368
  104.5 2.2 %inner.1 = bf16[8,256,128]{2,1,0:T(8,128)(2,1)} custom-call(bf16[8,528,128]{2,1,0:T(8,128)(2,1)} %all-to-all-done.2.parcels), custom_call_target="tpu_custom_call" | custom-call | flops 2162688 | bytes 2162688 | tf_op jit(solution)/shard_map/inner/pallas_call | solution.py:234
  106.8 3.5 %all-to-all-start.3 = ((bf16[8,256,128]{2,1,0:T(8,128)(2,1)}), bf16[8,256,128]{2,1,0:T(8,128)(2,1)S(1)}, u32[]{:S(2)}, u32[]{:S(2)}) async-start(bf16[8,256,128]{2,1,0:T(8,128)(2,1)} %inner.1), calls=%async_computation.3 | async-start | bytes 1048576 | tf_op jit(solution)/shard_map/all_to_all | solution.py:370
  110.3 5.4 %collective-permute-start.6 = (bf16[4,64,256]{2,1,0:T(8,128)(2,1)S(1)}, bf16[4,64,256]{2,1,0:T(8,128)(2,1)S(1)}, u32[]{:S(2)}, u32[]{:S(2)}) collective-permute-start(bf16[4,64,256]{2,1,0:T(8,128)(2,1)S(1)} %select_convert_fusion.1), channel_id=1, source_target_pairs={{0,8},{2,10},{4,12},{6,14},{8,0},{10,2},{12,4},{14,6},{1,9},{3,11}... | collective-permute-start | bytes 393224 | tf_op jit(solution)/shard_map/ppermute | solution.py:23
  115.7 18.1 %collective-permute-done.6 = bf16[4,64,256]{2,1,0:T(8,128)(2,1)S(1)} collective-permute-done((bf16[4,64,256]{2,1,0:T(8,128)(2,1)S(1)}, bf16[4,64,256]{2,1,0:T(8,128)(2,1)S(1)}, u32[]{:S(2)}, u32[]{:S(2)}) %collective-permute-start.6) | collective-permute-done | bytes 131104 | tf_op jit(solution)/shard_map/ppermute | solution.py:23
  134.8 2.7 %down.1 = (bf16[16,16,256]{2,1,0:T(8,128)(2,1)}, bf16[16,16,256]{2,1,0:T(8,128)(2,1)}) custom-call(s32[1]{0:T(128)} %bitcast.core, bf16[8,256,128]{2,1,0:T(8,128)(2,1)} %copy-done.2, bf16[4,1024,256]{2,1,0:T(8,128)(2,1)} %down_own.1, bf16[2,1024,256]{2,1,0:T(8,128)(2,1)} %collective-permute-done.12.down_par), custom_call_target="tpu_custom_call" | custom-call | flops 268435456 | bytes 2097152 | tf_op jit(solution)/shard_map/down/pallas_call | solution.py:258
  139.6 1.6 %pad_maximum_fusion.2 = bf16[16,32,256]{2,1,0:T(8,128)(2,1)} fusion(bf16[16,16,256]{2,1,0:T(8,128)(2,1)S(1)} %collective-permute-done.13, bf16[16,16,256]{2,1,0:T(8,128)(2,1)} %get-tuple-element.11), kind=kLoop, calls=%fused_computation.23 | loop fusion | flops 524288 | bytes 524288 | tf_op jit(solution)/shard_map/concatenate | solution.py:372
  141.2 3.5 %all-to-all-start.4 = ((bf16[16,32,256]{2,1,0:T(8,128)(2,1)}), bf16[16,32,256]{2,1,0:T(8,128)(2,1)S(1)}, u32[]{:S(2)}, u32[]{:S(2)}) async-start(bf16[16,32,256]{2,1,0:T(8,128)(2,1)} %pad_maximum_fusion.2), calls=%async_computation.4 | async-start | bytes 524288 | tf_op jit(solution)/shard_map/all_to_all | solution.py:373
  145.0 2.6 %collective-permute-done.8 = bf16[1,64,256]{2,1,0:T(8,128)(2,1)S(1)} collective-permute-done((bf16[1,64,256]{2,1,0:T(8,128)(2,1)S(1)}, bf16[1,64,256]{2,1,0:T(8,128)(2,1)S(1)}, u32[]{:S(2)}, u32[]{:S(2)}) %collective-permute-start.8) | collective-permute-done | bytes 32800 | tf_op jit(solution)/shard_map/ppermute | solution.py:23
  147.6 5.1 %all-to-all-done.4 = bf16[16,32,256]{2,1,0:T(8,128)(2,1)S(1)} async-done(((bf16[16,32,256]{2,1,0:T(8,128)(2,1)}), bf16[16,32,256]{2,1,0:T(8,128)(2,1)S(1)}, u32[]{:S(2)}, u32[]{:S(2)}) %all-to-all-start.4) | async-done | bytes 262176 | tf_op jit(solution)/shard_map/all_to_all | solution.py:373
  (87 shorter events, 21.0 us)
Async XLA Ops:
  0.6 77.3 %copy-start = (bf16[4096,64]{0,1:T(8,128)(2,1)S(1)}, bf16[4096,64]{0,1:T(8,128)(2,1)}, u32[]{:S(2)}) copy-start(bf16[4096,64]{0,1:T(8,128)(2,1)} %param.39) | copy-start | bytes 1572868
  5.0 4.6 %collective-permute-start = (bf16[8,64,256]{2,1,0:T(8,128)(2,1)}, bf16[8,64,256]{2,1,0:T(8,128)(2,1)S(1)}, u32[]{:S(2)}, u32[]{:S(2)}) collective-permute-start(bf16[8,64,256]{2,1,0:T(8,128)(2,1)} %get-tuple-element.10), channel_id=1, source_target_pairs={{0,1},{1,0},{2,3},{3,2},{4,5},{5,4},{6,7},{7,6},{8,9},{9,8},{10,11... | collective-permute-start | bytes 786440 | tf_op jit(solution)/shard_map/ppermute | solution.py:19
  9.3 10.5 %copy-start.8 = (s32[64,4]{0,1:T(4,128)S(1)}, s32[64,4]{0,1:T(4,128)}, u32[]{:S(2)}) copy-start(s32[64,4]{0,1:T(4,128)} %param.44) | copy-start | bytes 3076
  9.3 53.1 %collective-permute-start.10 = (bf16[2,256,1024]{2,1,0:T(8,128)(2,1)}, bf16[2,256,1024]{2,1,0:T(8,128)(2,1)S(1)}, u32[]{:S(2)}, u32[]{:S(2)}) collective-permute-start(bf16[2,256,1024]{2,1,0:T(8,128)(2,1)} %constant_dynamic-slice_fusion.2), channel_id=1, source_target_pairs={{0,1},{1,0},{2,3},{3,2},{4,5},{5,4},{6,7},{7,6},{8,9},{9,8},{10,11... | collective-permute-start | bytes 3145736 | tf_op jit(solution)/shard_map/ppermute | solution.py:19
  10.4 17.6 %all-to-all-start = ((bf16[8,64,256]{2,1,0:T(8,128)(2,1)}), bf16[8,64,256]{2,1,0:T(8,128)(2,1)S(1)}, u32[]{:S(2)}, u32[]{:S(2)}) async-start(bf16[8,64,256]{2,1,0:T(8,128)(2,1)} %add_convert_fusion), calls=%async_computation | async-start | bytes 524288 | tf_op jit(solution)/shard_map/all_to_all | solution.py:331
  19.1 43.3 %collective-permute-start.11 = (bf16[2,256,1024]{2,1,0:T(8,128)(2,1)}, bf16[2,256,1024]{2,1,0:T(8,128)(2,1)S(1)}, u32[]{:S(2)}, u32[]{:S(2)}) collective-permute-start(bf16[2,256,1024]{2,1,0:T(8,128)(2,1)} %constant_dynamic-slice_fusion.1), channel_id=1, source_target_pairs={{0,1},{1,0},{2,3},{3,2},{4,5},{5,4},{6,7},{7,6},{8,9},{9,8},{10,11... | collective-permute-start | bytes 3145736 | tf_op jit(solution)/shard_map/ppermute | solution.py:19
  28.8 33.0 %copy-start.7 = (f32[4096]{0:T(1024)S(1)}, f32[4096]{0:T(1024)}, u32[]{:S(2)}) copy-start(f32[4096]{0:T(1024)} %param.25) | copy-start | bytes 49156
  28.8 2.9 %collective-permute-start.1 = (bf16[1,64,256]{2,1,0:T(8,128)(2,1)S(1)}, bf16[1,64,256]{2,1,0:T(8,128)(2,1)S(1)}, u32[]{:S(2)}, u32[]{:S(2)}) collective-permute-start(bf16[1,64,256]{2,1,0:T(8,128)(2,1)S(1)} %bitcast.103), channel_id=1, source_target_pairs={{0,2},{2,0},{4,6},{6,4},{8,10},{10,8},{12,14},{14,12},{1,3},{3,1},... | collective-permute-start | bytes 98312 | tf_op jit(solution)/shard_map/ppermute | solution.py:23
  31.7 4.5 %collective-permute-start.2 = (bf16[2,64,256]{2,1,0:T(8,128)(2,1)S(1)}, bf16[2,64,256]{2,1,0:T(8,128)(2,1)S(1)}, u32[]{:S(2)}, u32[]{:S(2)}) collective-permute-start(bf16[2,64,256]{2,1,0:T(8,128)(2,1)S(1)} %maximum_bitcast_fusion), channel_id=1, source_target_pairs={{0,4},{2,6},{4,0},{6,2},{8,12},{10,14},{12,8},{14,10},{1,5},{3,7},... | collective-permute-start | bytes 196616 | tf_op jit(solution)/shard_map/ppermute | solution.py:23
  36.2 8.5 %collective-permute-start.3 = (bf16[4,64,256]{2,1,0:T(8,128)(2,1)S(1)}, bf16[4,64,256]{2,1,0:T(8,128)(2,1)S(1)}, u32[]{:S(2)}, u32[]{:S(2)}) collective-permute-start(bf16[4,64,256]{2,1,0:T(8,128)(2,1)S(1)} %bitcast.102), channel_id=1, source_target_pairs={{0,8},{2,10},{4,12},{6,14},{8,0},{10,2},{12,4},{14,6},{1,9},{3,11}... | collective-permute-start | bytes 393224 | tf_op jit(solution)/shard_map/ppermute | solution.py:23
  38.0 14.3 %all-to-all-start.1 = ((bf16[16,32,256]{2,1,0:T(8,128)(2,1)}), bf16[16,32,256]{2,1,0:T(8,128)(2,1)S(1)}, u32[]{:S(2)}, u32[]{:S(2)}) async-start(bf16[16,32,256]{2,1,0:T(8,128)(2,1)} %bitcast.27), calls=%async_computation.1 | async-start | bytes 524288 | tf_op jit(solution)/shard_map/all_to_all | solution.py:353
  44.8 29.6 %collective-permute-start.4 = (bf16[8,64,256]{2,1,0:T(8,128)(2,1)S(1)}, bf16[8,64,256]{2,1,0:T(8,128)(2,1)S(1)}, u32[]{:S(2)}, u32[]{:S(2)}) collective-permute-start(bf16[8,64,256]{2,1,0:T(8,128)(2,1)S(1)} %bitcast.101), channel_id=1, source_target_pairs={{0,1},{1,0},{2,3},{3,2},{4,5},{5,4},{6,7},{7,6},{8,9},{9,8},{10,11... | collective-permute-start | bytes 786440 | tf_op jit(solution)/shard_map/ppermute | solution.py:19
  52.3 10.1 %copy-start.3 = (bf16[16,32,256]{2,1,0:T(8,128)(2,1)}, bf16[16,32,256]{2,1,0:T(8,128)(2,1)S(1)}, u32[]{:S(2)}) copy-start(bf16[16,32,256]{2,1,0:T(8,128)(2,1)S(1)} %all-to-all-done.1) | copy-start | bytes 786436
  53.0 9.4 %collective-permute-start.9 = (bf16[16,1,2,8,256]{4,3,2,1,0:T(8,128)(2,1)}, bf16[16,1,2,8,256]{4,3,2,1,0:T(8,128)(2,1)}, u32[]{:S(2)}, u32[]{:S(2)}) collective-permute-start(bf16[16,1,2,8,256]{4,3,2,1,0:T(8,128)(2,1)} %slice.67), channel_id=1, source_target_pairs={{0,1},{1,0},{2,3},{3,2},{4,5},{5,4},{6,7},{7,6},{8,9},{9,8},{10,11... | collective-permute-start | bytes 393224 | tf_op jit(solution)/shard_map/ppermute | solution.py:19
  67.5 37.0 %all-to-all-start.2 = ((bf16[8,528,128]{2,1,0:T(8,128)(2,1)}), bf16[8,528,128]{2,1,0:T(8,128)(2,1)}, u32[]{:S(2)}, u32[]{:S(2)}) async-start(bf16[8,528,128]{2,1,0:T(8,128)(2,1)} %gate_up.1), calls=%async_computation.2 | async-start | bytes 2162688 | tf_op jit(solution)/shard_map/all_to_all | solution.py:368
  79.8 2.2 %collective-permute-start.5 = (bf16[8,64,256]{2,1,0:T(8,128)(2,1)S(1)}, bf16[8,64,256]{2,1,0:T(8,128)(2,1)S(1)}, u32[]{:S(2)}, u32[]{:S(2)}) collective-permute-start(bf16[8,64,256]{2,1,0:T(8,128)(2,1)S(1)} %fusion.6), channel_id=1, source_target_pairs={{0,1},{1,0},{2,3},{3,2},{4,5},{5,4},{6,7},{7,6},{8,9},{9,8},{10,11... | collective-permute-start | bytes 786440 | tf_op jit(solution)/shard_map/ppermute | solution.py:19
  81.5 52.5 %collective-permute-start.12 = (bf16[2,1024,256]{2,1,0:T(8,128)(2,1)S(1)}, bf16[2,1024,256]{2,1,0:T(8,128)(2,1)}, u32[]{:S(2)}, u32[]{:S(2)}) collective-permute-start(bf16[2,1024,256]{2,1,0:T(8,128)(2,1)S(1)} %constant_dynamic-slice_fusion), channel_id=1, source_target_pairs={{0,1},{1,0},{2,3},{3,2},{4,5},{5,4},{6,7},{7,6},{8,9},{9,8},{10,11... | collective-permute-start | bytes 3145736 | tf_op jit(solution)/shard_map/ppermute | solution.py:19
  82.0 33.7 %copy-start.9 = (f32[64,4]{0,1:T(4,128)S(1)}, f32[64,4]{0,1:T(4,128)}, u32[]{:S(2)}) copy-start(f32[64,4]{0,1:T(4,128)} %param.45) | copy-start | bytes 3076
  106.8 27.2 %all-to-all-start.3 = ((bf16[8,256,128]{2,1,0:T(8,128)(2,1)}), bf16[8,256,128]{2,1,0:T(8,128)(2,1)S(1)}, u32[]{:S(2)}, u32[]{:S(2)}) async-start(bf16[8,256,128]{2,1,0:T(8,128)(2,1)} %inner.1), calls=%async_computation.3 | async-start | bytes 1048576 | tf_op jit(solution)/shard_map/all_to_all | solution.py:370
  110.3 23.5 %collective-permute-start.6 = (bf16[4,64,256]{2,1,0:T(8,128)(2,1)S(1)}, bf16[4,64,256]{2,1,0:T(8,128)(2,1)S(1)}, u32[]{:S(2)}, u32[]{:S(2)}) collective-permute-start(bf16[4,64,256]{2,1,0:T(8,128)(2,1)S(1)} %select_convert_fusion.1), channel_id=1, source_target_pairs={{0,8},{2,10},{4,12},{6,14},{8,0},{10,2},{12,4},{14,6},{1,9},{3,11}... | collective-permute-start | bytes 393224 | tf_op jit(solution)/shard_map/ppermute | solution.py:23
  133.8 4.6 %collective-permute-start.7 = (bf16[2,64,256]{2,1,0:T(8,128)(2,1)S(1)}, bf16[2,64,256]{2,1,0:T(8,128)(2,1)S(1)}, u32[]{:S(2)}, u32[]{:S(2)}) collective-permute-start(bf16[2,64,256]{2,1,0:T(8,128)(2,1)S(1)} %select_convert_fusion.2), channel_id=1, source_target_pairs={{0,4},{2,6},{4,0},{6,2},{8,12},{10,14},{12,8},{14,10},{1,5},{3,7},... | collective-permute-start | bytes 196616 | tf_op jit(solution)/shard_map/ppermute | solution.py:23
  137.4 2.1 %collective-permute-start.13 = (bf16[16,16,256]{2,1,0:T(8,128)(2,1)}, bf16[16,16,256]{2,1,0:T(8,128)(2,1)S(1)}, u32[]{:S(2)}, u32[]{:S(2)}) collective-permute-start(bf16[16,16,256]{2,1,0:T(8,128)(2,1)} %get-tuple-element.12), channel_id=1, source_target_pairs={{0,1},{1,0},{2,3},{3,2},{4,5},{5,4},{6,7},{7,6},{8,9},{9,8},{10,11... | collective-permute-start | bytes 393224 | tf_op jit(solution)/shard_map/ppermute | solution.py:19
  141.2 11.6 %all-to-all-start.4 = ((bf16[16,32,256]{2,1,0:T(8,128)(2,1)}), bf16[16,32,256]{2,1,0:T(8,128)(2,1)S(1)}, u32[]{:S(2)}, u32[]{:S(2)}) async-start(bf16[16,32,256]{2,1,0:T(8,128)(2,1)} %pad_maximum_fusion.2), calls=%async_computation.4 | async-start | bytes 524288 | tf_op jit(solution)/shard_map/all_to_all | solution.py:373
  144.8 2.9 %collective-permute-start.8 = (bf16[1,64,256]{2,1,0:T(8,128)(2,1)S(1)}, bf16[1,64,256]{2,1,0:T(8,128)(2,1)S(1)}, u32[]{:S(2)}, u32[]{:S(2)}) collective-permute-start(bf16[1,64,256]{2,1,0:T(8,128)(2,1)S(1)} %select_convert_fusion.3), channel_id=1, source_target_pairs={{0,2},{2,0},{4,6},{6,4},{8,10},{10,8},{12,14},{14,12},{1,3},{3,1},... | collective-permute-start | bytes 98312 | tf_op jit(solution)/shard_map/ppermute | solution.py:23
  (5 other events, 15.3 us)
